TPU v7x, 256 devices: a whole 4x4x8 slice. The times are simulated.
256 devices in a mesh: sp: 64 (over z, y, core), tp: 4 (over x).
Axes of the slice: x: 4, y: 4, z: 8, core: 2. Of those that a mesh axis runs over, the one named last changes fastest.
Arguments:
- hidden_state: bfloat16 [8192, 2048], P('sp'), may hold values from -125 to 125
- norm_gain: float32 [2048], replicated, may hold values from 0.1 to 1.9
- route_ids: int32 [8192, 2], P('sp'), may hold values from 0 to 63, all different within a row; in each aligned block of 128 rows (0 to 127, 128 to 255, ...) at most 8 rows name the same one
- route_logits: float32 [8192, 2], P('sp'), may hold values from -6 to 6
- cotangent: bfloat16 [8192, 2048], P('sp'), may hold values from -16 to 16
- w_gate: bfloat16 [64, 2048, 1536], P('sp', None, 'tp'), may hold values from -0.125 to 0.125
- w_up: bfloat16 [64, 2048, 1536], P('sp', None, 'tp'), may hold values from -0.125 to 0.125
- w_down: bfloat16 [64, 1536, 2048], P('sp', 'tp'), may hold values from -0.15625 to 0.15625
- w_out: bfloat16 [2048, 1024], P(None, 'tp'), may hold values from -0.1875 to 0.1875
- query_rows: bfloat16 [8192, 512], P('sp', 'tp'), may hold values from -6 to 6
- key_rows: bfloat16 [8192, 512], P('sp', 'tp'), may hold values from -6 to 6
- value_rows: bfloat16 [8192, 1024], P('sp', 'tp'), may hold values from -6 to 6
- log_decay: float32 [8192, 512], P('sp', 'tp'), may hold values from -1.6 to 0
- head_gain: float32 [1024], P('tp'), may hold values from 0.1 to 1.9
Outputs:
- d_w_gate: bfloat16 [64, 2048, 1536], P('sp', None, 'tp')
- d_w_up: bfloat16 [64, 2048, 1536], P('sp', None, 'tp')
- d_w_down: bfloat16 [64, 1536, 2048], P('sp', 'tp')
- d_w_out: float32 [2048, 1024], P('sp', 'tp')
- d_queries: bfloat16 [8192, 512], P('sp', 'tp')
- d_keys: bfloat16 [8192, 512], P('sp', 'tp')
- d_values: bfloat16 [8192, 1024], P('sp', 'tp')
- d_log_decay: float32 [8192, 512], P('sp', 'tp')
Inputs may be any that keep to these rules, and one draw needn't show every extreme that they name: `route_ids`: in the rows of one device each expert is named at most 8 times, a bound that some block reaches; the two experts of a position differ.
All inputs are finite; a program needn't handle non-finite values.
Results may differ from a plain program's by a relative error of at most 0.014.
Values may be sent and summed in bfloat16 or wider, within the bound.
No kernel may reach another device: no remote copies, remote signals or barrier semaphores. Data moves between devices by JAX's collectives and lax.ppermute only.
A program may use at most 128 MiB of HBM per device.

v0:
```python
import jax
import jax.numpy as jnp
from jax import lax
from jax.sharding import Mesh
from jax.sharding import PartitionSpec as P

KEY_DIM = 64
VAL_DIM = 128
BLOCK = 64
SP = ("sp_0", "sp_1", "sp_2")


exact_numeric_mode = lax.Precision.HIGHEST
eps_value = 1e-06


def filled_with(array, identity):
    return jax.tree.map(
        lambda a, e: jnp.broadcast_to(jnp.asarray(e, a.dtype), a.shape), array, identity
    )


def collected_together(array, axis):
    leaves = jax.tree.leaves(array)
    sequence = sorted(range(len(leaves)), key=lambda k: -leaves[k].size)
    width = (1, *leaves[sequence[0]].shape)[-1]
    lines = [
        jnp.pad(leaves[k].reshape(-1), (0, -leaves[k].size % width)).reshape(-1, width)
        for k in sequence
    ]
    both, at, found = (lax.all_gather(jnp.concatenate(lines), axis), 0, {})
    for k, line in zip(sequence, lines):
        section = both[:, at : at + len(line)].reshape(len(both), -1)
        found[k] = section[:, : leaves[k].size].reshape(-1, *leaves[k].shape)
        at += len(line)
    numbers = iter(range(len(leaves)))
    return jax.tree.map(lambda _: found[next(numbers)], array)


def carried_in(array, axes, combine, identity, reverse):
    before = start = filled_with(array, identity)
    so_far = array
    for axis in reversed(axes):
        length, position = (lax.axis_size(axis), lax.axis_index(axis))
        pieces = collected_together(so_far, axis)
        inside, so_far = (start, start)
        for k in reversed(range(length)) if reverse else range(length):
            passed = k > position if reverse else k < position
            so_far = combine(so_far, jax.tree.map(lambda part: part[k], pieces))
            inside = jax.tree.map(lambda new, old: jnp.where(passed, new, old), so_far, inside)
        before = combine(inside, before)
    return before


def side_by_side(arrays, axis, split_dim, concat_dim, along):
    both = jnp.concatenate(arrays, axis=along)
    result, at, gathered = (
        lax.all_to_all(both, axis, split_axis=split_dim, concat_axis=concat_dim, tiled=True),
        0,
        [],
    )
    for a in arrays:
        gathered.append(lax.slice_in_dim(result, at, at + a.shape[along], axis=along))
        at += a.shape[along]
    return tuple(gathered)


def side_by_side_2(arrays, axis, dim, along):
    widths = [a.shape[along] for a in arrays]
    both = jnp.concatenate(arrays, axis=along)
    result = lax.all_gather(both, axis, axis=dim, tiled=True)
    return tuple(jnp.split(result, [sum(widths[:k]) for k in range(1, len(widths))], axis=along))


def split_up(array, dim, length):
    dims = array.shape
    blocks = array.reshape(*dims[:dim], length, dims[dim] // length, *dims[dim + 1 :])
    return jnp.moveaxis(blocks, dim, 0)


def sent_and_summed(array, axis, dim):
    length = lax.axis_size(axis)
    blocks = lax.all_to_all(split_up(array, dim, length), axis, 0, 0, tiled=True)
    return jnp.sum(blocks.astype(jnp.float32), axis=0)


def joined_along(blocks, dim):
    blocks = jnp.moveaxis(blocks, 0, dim)
    dims = blocks.shape
    return blocks.reshape(*dims[:dim], dims[dim] * dims[dim + 1], *dims[dim + 2 :])


def from_everyone(array, axis):
    copies = jnp.broadcast_to(array, (lax.axis_size(axis), *array.shape))
    return lax.all_to_all(copies, axis, split_axis=0, concat_axis=0, tiled=True)


def gathered_copies(array, axis, dim):
    return joined_along(from_everyone(array, axis), dim)


def own_rows(so_far, axes):
    for axis in axes:
        so_far = lax.psum_scatter(so_far, axis, scatter_dimension=0, tiled=True)
    return so_far


def chain_forward(earlier, later):
    return (earlier[0] * later[0], later[0][:, :, None] * earlier[1] + later[1])


def chain_backward(earlier, later):
    return (earlier[0] * later[0], later[1] + later[0][:, :, None] * earlier[1])


def carry_blocks(carried_state, inputs):
    decay_now, term_now = inputs
    return (decay_now[:, :, None] * carried_state + term_now, carried_state)


def body(
    hidden_state,
    norm_gain,
    route_ids,
    route_logits,
    cotangent,
    w_gate,
    w_up,
    w_down,
    w_out,
    query_rows,
    key_rows,
    value_rows,
    log_decay,
    head_gain,
):
    tok_count, model_width = hidden_state.shape
    head_count = head_gain.shape[0] // VAL_DIM
    block_count = tok_count // BLOCK
    shape_key = (block_count, BLOCK, head_count, KEY_DIM)
    shape_value = (block_count, BLOCK, head_count, VAL_DIM)
    query_f = query_rows.astype(jnp.float32).reshape(shape_key)
    key_f = key_rows.astype(jnp.float32).reshape(shape_key)
    value_f = value_rows.astype(jnp.float32).reshape(shape_value)
    cumulative_decay = jnp.cumsum(log_decay.reshape(shape_key), axis=1)
    decay_mid = cumulative_decay[:, BLOCK // 2 : BLOCK // 2 + 1]
    final_decay = cumulative_decay[:, BLOCK - 1 : BLOCK]
    query_in = query_f * jnp.exp(cumulative_decay - decay_mid)
    key_in = key_f * jnp.exp(decay_mid - cumulative_decay)
    key_end = key_f * jnp.exp(final_decay - cumulative_decay)
    query_start = query_f * jnp.exp(cumulative_decay)
    causal = (jnp.arange(BLOCK)[:, None] >= jnp.arange(BLOCK)[None, :])[None, None]
    last_logs = final_decay[:, 0]
    through = jnp.cumsum(last_logs, axis=0)
    total_log = through[-1]
    total_decay = jnp.exp(total_log)
    block_decay = jnp.exp(last_logs)
    block_kv = jnp.einsum("bshk,bshv->bhkv", key_end, value_f, precision=exact_numeric_mode)
    zero_state = jnp.zeros((head_count, KEY_DIM, VAL_DIM), jnp.float32)
    ones_decay = jnp.ones_like(total_log)
    local_end, local_start = lax.scan(carry_blocks, zero_state, (block_decay, block_kv))
    ahead = carried_in((total_decay, local_end), SP, chain_forward, (ones_decay, zero_state), False)
    state_in = ahead[1]
    block_states = local_start + jnp.exp(through - last_logs)[:, :, :, None] * state_in
    end_state = total_decay[:, :, None] * state_in + local_end
    scores = jnp.where(
        causal, jnp.einsum("bthk,bshk->bhts", query_in, key_in, precision=exact_numeric_mode), 0.0
    )
    head_out = jnp.einsum("bhts,bshv->bthv", scores, value_f, precision=exact_numeric_mode)
    head_out = head_out + jnp.einsum(
        "bthk,bhkv->bthv", query_start, block_states, precision=exact_numeric_mode
    )
    inv_rms = lax.rsqrt(jnp.mean(head_out * head_out, axis=-1, keepdims=True) + eps_value)
    normed = head_out * inv_rms
    gain_heads = head_gain.reshape(head_count, VAL_DIM)
    mixed_out = (normed * gain_heads).reshape(tok_count, head_count * VAL_DIM).astype(jnp.bfloat16)
    state_f = hidden_state.astype(jnp.float32)
    row_scale = lax.rsqrt(jnp.mean(state_f * state_f, axis=-1, keepdims=True) + eps_value)
    unit_rows = state_f * row_scale
    normed_in = (unit_rows * norm_gain).astype(jnp.bfloat16)
    route_weight = jax.nn.softmax(route_logits, axis=-1)
    cot_f = cotangent.astype(jnp.float32)
    slot_grads = (
        (route_weight[:, :, None] * cot_f[:, None, :])
        .astype(jnp.bfloat16)
        .reshape(2 * tok_count, model_width)
    )
    expert_count = lax.axis_size(SP)
    capacity = 4 * tok_count // expert_count
    flat_ids = route_ids.reshape(-1)
    one_hot = (flat_ids[:, None] == jnp.arange(expert_count, dtype=jnp.int32)[None, :]).astype(
        jnp.int32
    )
    slot_rank = jnp.sum((jnp.cumsum(one_hot, axis=0) - 1) * one_hot, axis=1)
    slot_of = flat_ids * capacity + slot_rank
    source = (
        jnp.full((expert_count * capacity,), 2 * tok_count, jnp.int32)
        .at[slot_of]
        .set(jnp.arange(2 * tok_count, dtype=jnp.int32))
    )
    token_of = jnp.where(source < 2 * tok_count, source // 2, tok_count)
    padded_in = jnp.concatenate([normed_in, jnp.zeros((1, model_width), jnp.bfloat16)], axis=0)
    padded_grad = jnp.concatenate([slot_grads, jnp.zeros((1, model_width), jnp.bfloat16)], axis=0)
    send_in = padded_in[token_of].reshape(expert_count, capacity, model_width)
    send_grad = padded_grad[source].reshape(expert_count, capacity, model_width)
    part_width = model_width // lax.axis_size("tp")
    feature_start = lax.axis_index("tp") * part_width
    part_in = lax.dynamic_slice_in_dim(send_in, feature_start, part_width, 2)
    part_grad = lax.dynamic_slice_in_dim(send_grad, feature_start, part_width, 2)
    part_in, part_grad = side_by_side((part_in, part_grad), SP, 0, 0, 1)
    got_in, got_grad = side_by_side_2((part_in, part_grad), "tp", 2, 0)
    rows_in = got_in.reshape(-1, model_width)
    rows_grad = got_grad.reshape(-1, model_width)
    gate_w = w_gate[0]
    up_w = w_up[0]
    down_w = w_down[0]
    gate_pre = jnp.dot(rows_in, gate_w, preferred_element_type=jnp.float32)
    up_pre = jnp.dot(rows_in, up_w, preferred_element_type=jnp.float32)
    gate_sig = jax.nn.sigmoid(gate_pre)
    silu_gate = gate_pre * gate_sig
    hidden_units = (silu_gate * up_pre).astype(jnp.bfloat16)
    grad_down = jnp.einsum("rf,rd->fd", hidden_units, rows_grad, preferred_element_type=jnp.float32)
    grad_hidden = jnp.einsum("rd,fd->rf", rows_grad, down_w, preferred_element_type=jnp.float32)
    grad_gate_pre = (grad_hidden * up_pre * gate_sig * (1.0 + gate_pre * (1.0 - gate_sig))).astype(
        jnp.bfloat16
    )
    grad_up_pre = (grad_hidden * silu_gate).astype(jnp.bfloat16)
    grad_gate_w = jnp.einsum(
        "rd,rf->df", rows_in, grad_gate_pre, preferred_element_type=jnp.float32
    )
    grad_up_w = jnp.einsum("rd,rf->df", rows_in, grad_up_pre, preferred_element_type=jnp.float32)
    partial_rows = jnp.einsum(
        "rf,df->rd", grad_gate_pre, gate_w, preferred_element_type=jnp.float32
    )
    partial_rows = partial_rows + jnp.einsum(
        "rf,df->rd", grad_up_pre, up_w, preferred_element_type=jnp.float32
    )
    partial_rows = partial_rows.reshape(expert_count, capacity, model_width)
    summed = sent_and_summed(partial_rows.astype(jnp.bfloat16), "tp", 2).astype(jnp.bfloat16)
    returned = lax.all_to_all(summed, SP, split_axis=0, concat_axis=0, tiled=True)
    picked = returned.reshape(-1, part_width)[slot_of].reshape(tok_count, 2, part_width)
    picked = gathered_copies(picked, "tp", 2)
    grad_normed = jnp.sum(picked.astype(jnp.float32), axis=1)
    grad_unit = grad_normed * norm_gain
    grad_state = row_scale * (
        grad_unit - unit_rows * jnp.mean(grad_unit * unit_rows, axis=-1, keepdims=True)
    )
    grad_mixed = (cot_f + grad_state).astype(jnp.bfloat16)
    grad_out_w = own_rows(
        jnp.einsum("td,th->dh", grad_mixed, mixed_out, preferred_element_type=jnp.float32), SP
    )
    grad_mix = jnp.dot(grad_mixed, w_out, preferred_element_type=jnp.float32).astype(jnp.bfloat16)
    grad_mix = lax.optimization_barrier(grad_mix).astype(jnp.float32).reshape(shape_value)
    grad_scaled = grad_mix * gain_heads
    grad_out = inv_rms * (
        grad_scaled - normed * jnp.mean(grad_scaled * normed, axis=-1, keepdims=True)
    )
    block_adj = jnp.einsum("bthk,bthv->bhkv", query_start, grad_out, precision=exact_numeric_mode)
    local_adj, later_adj = lax.scan(
        carry_blocks, zero_state, (block_decay, block_adj), reverse=True
    )
    behind = carried_in(
        (total_decay, local_adj), SP, chain_backward, (ones_decay, zero_state), True
    )
    adj_end = behind[1]
    block_adj_end = later_adj + jnp.exp(total_log - through)[:, :, :, None] * adj_end
    grad_dots = jnp.where(
        causal, jnp.einsum("bthv,bshv->bhts", grad_out, value_f, precision=exact_numeric_mode), 0.0
    )
    grad_query = jnp.exp(cumulative_decay - decay_mid) * jnp.einsum(
        "bhts,bshk->bthk", grad_dots, key_in, precision=exact_numeric_mode
    )
    grad_query = grad_query + jnp.exp(cumulative_decay) * jnp.einsum(
        "bthv,bhkv->bthk", grad_out, block_states, precision=exact_numeric_mode
    )
    grad_key = jnp.exp(decay_mid - cumulative_decay) * jnp.einsum(
        "bhts,bthk->bshk", grad_dots, query_in, precision=exact_numeric_mode
    )
    grad_key = grad_key + jnp.exp(final_decay - cumulative_decay) * jnp.einsum(
        "bhkv,bshv->bshk", block_adj_end, value_f, precision=exact_numeric_mode
    )
    grad_value = jnp.einsum("bhts,bthv->bshv", scores, grad_out, precision=exact_numeric_mode)
    grad_value = grad_value + jnp.einsum(
        "bshk,bhkv->bshv", key_end, block_adj_end, precision=exact_numeric_mode
    )
    log_terms = (query_f * grad_query - key_f * grad_key).reshape(tok_count, head_count * KEY_DIM)
    suffix = lax.cumsum(log_terms, axis=0, reverse=True)
    tail_term = jnp.sum(adj_end * end_state, axis=-1).reshape(1, head_count * KEY_DIM)
    grad_log = suffix + tail_term
    return (
        grad_gate_w.astype(jnp.bfloat16)[None],
        grad_up_w.astype(jnp.bfloat16)[None],
        grad_down.astype(jnp.bfloat16)[None],
        grad_out_w,
        grad_query.reshape(tok_count, -1).astype(jnp.bfloat16),
        grad_key.reshape(tok_count, -1).astype(jnp.bfloat16),
        grad_value.reshape(tok_count, -1).astype(jnp.bfloat16),
        grad_log,
    )


def solution(mesh):
    split = Mesh(mesh.devices.reshape(8, 4, 2, mesh.shape["tp"]), ("sp_0", "sp_1", "sp_2", "tp"))
    in_specs = (
        P(SP, None),
        P(),
        P(SP, None),
        P(SP, None),
        P(SP, None),
        P(SP, None, "tp"),
        P(SP, None, "tp"),
        P(SP, "tp", None),
        P(None, "tp"),
        P(SP, "tp"),
        P(SP, "tp"),
        P(SP, "tp"),
        P(SP, "tp"),
        P("tp"),
    )
    out_specs = (
        P(SP, None, "tp"),
        P(SP, None, "tp"),
        P(SP, "tp", None),
        P(SP, "tp"),
        P(SP, "tp"),
        P(SP, "tp"),
        P(SP, "tp"),
        P(SP, "tp"),
    )
    return jax.shard_map(body, mesh=split, in_specs=in_specs, out_specs=out_specs, check_vma=False)
```

profile of v0, /device:TPU:1, one launch (start us, length us, event | category | flops | bytes accessed | tf_op | source)
XLA Modules:
  0.0 315.0 jit_solution(17117928363213554804)
XLA Ops:
  7.2 0.8 broadcast_multiply_fusion.5
  8.0 0.8 copy.97
  9.1 3.4 %mul.928 = f32[128,2,2048]{2,1,0:T(2,128)} broadcast(bf16[128,2048]{1,0:T(8,128)(2,1)} %param.22), dimensions={0,2} | broadcast | bytes 2621440 | tf_op jit(solution)/shard_map/mul | solution.py:184
  12.5 3.8 %mul.929 = f32[256,2048]{1,0:T(8,128)} reshape(f32[128,2,2048]{2,1,0:T(2,128)} %mul.928) | data formatting | bytes 4194304 | tf_op jit(solution)/shard_map/mul | solution.py:184
  17.8 1.4 scatter_custom_fusion
  19.5 1.8 multiply_convert_fusion
  21.7 3.3 %gather_fusion.1 = bf16[512,2048]{1,0:T(8,128)(2,1)} fusion(bf16[257,2048]{1,0:T(8,128)(2,1)S(1)} %concatenate.31, s32[1024]{0:T(1024)S(1)} %get-tuple-element.303), kind=kCustom, calls=%fused_computation.1 | custom fusion | bytes 4196352 | tf_op jit(solution)/shard_map/gather | solution.py:205
  25.0 1.1 constant_dynamic-slice_fusion
  26.1 3.3 %gather_fusion = bf16[512,2048]{1,0:T(8,128)(2,1)} fusion(bf16[129,2048]{1,0:T(8,128)(2,1)S(1)} %concatenate.30, s32[1024]{0:T(1024)S(1)} %get-tuple-element.304), kind=kCustom, calls=%fused_computation | custom fusion | bytes 4196352 | tf_op jit(solution)/shard_map/gather | solution.py:204
  29.5 1.1 constant_dynamic-slice_fusion.1
  30.7 41.1 %all_to_all.20 = bf16[64,16,512]{2,1,0:T(8,128)(2,1)S(1)} all-to-all(bf16[64,16,512]{2,1,0:T(8,128)(2,1)S(1)} %pad_maximum_fusion), channel_id=1, replica_groups=mesh['sp_0'=8,'sp_1'=4,'sp_2'=2,'tp'=4] {'sp_0','sp_1','sp_2'}, dimensions={0} | all-to-all | bytes 2097152 | tf_op jit(solution)/shard_map/all_to_all | solution.py:58
  71.9 1.1 pad_maximum_fusion.1
  75.0 2.7 all-gather.6
  77.9 10.4 %all-gather.7 = f32[4,129,128]{2,1,0:T(8,128)S(1)} all-gather(f32[1,129,128]{2,1,0:T(8,128)S(1)} %maximum_bitcast_fusion), channel_id=3, replica_groups=mesh['sp_0'=8,'sp_1'=4,'sp_2'=2,'tp'=4] {'sp_1'}, dimensions={0}, use_global_device_ids=true | all-gather | bytes 330240 | tf_op jit(solution)/shard_map/all_gather | solution.py:31
  90.1 22.2 %all-gather.8 = f32[8,129,128]{2,1,0:T(8,128)S(1)} all-gather(f32[1,129,128]{2,1,0:T(8,128)S(1)} %maximum_bitcast_fusion.1), channel_id=4, replica_groups=mesh['sp_0'=8,'sp_1'=4,'sp_2'=2,'tp'=4] {'sp_0'}, dimensions={0}, use_global_device_ids=true | all-gather | bytes 594432 | tf_op jit(solution)/shard_map/all_gather | solution.py:31
  112.3 8.3 %all-gather.14.cloned.1.call-done = bf16[128,8,2048]{2,1,0:T(8,128)(2,1)} async-done(((bf16[128,8,512]{2,1,0:T(8,128)(2,1)}), bf16[128,8,2048]{2,1,0:T(8,128)(2,1)}) %all-gather.14.cloned.1.call-update) | async-done | bytes 4194320 | tf_op jit(solution)/shard_map/all_gather | solution.py:71
  120.6 3.0 fusion.6
  123.9 1.3 fusion.9
  125.6 1.4 multiply_convert_fusion.2
  127.1 1.3 fusion.4
  128.4 1.3 add_convert_fusion
  129.7 1.5 copy.160
  131.2 4.6 %all-to-all-start.1 = ((bf16[4,64,8,512]{3,2,1,0:T(8,128)(2,1)}), bf16[4,64,8,512]{3,2,1,0:T(8,128)(2,1)}, u32[]{:S(2)}, u32[]{:S(2)}) async-start(bf16[4,64,8,512]{3,2,1,0:T(8,128)(2,1)} %bitcast.286), calls=%async_computation.1 | async-start | bytes 4194304 | tf_op jit(solution)/shard_map/all_to_all | solution.py:83
  142.1 1.1 add_add_fusion
  143.2 18.3 %all-to-all-done.1 = bf16[4,64,8,512]{3,2,1,0:T(8,128)(2,1)} async-done(((bf16[4,64,8,512]{3,2,1,0:T(8,128)(2,1)}), bf16[4,64,8,512]{3,2,1,0:T(8,128)(2,1)}, u32[]{:S(2)}, u32[]{:S(2)}) %all-to-all-start.1) | async-done | bytes 2097184 | tf_op jit(solution)/shard_map/all_to_all | solution.py:83
  161.4 2.9 reduce_sum.94
  164.3 11.7 %all-to-all-start.2 = ((bf16[64,8,512]{2,1,0:T(8,128)(2,1)}), bf16[64,8,512]{2,1,0:T(8,128)(2,1)S(1)}, u32[]{:S(2)}, u32[]{:S(2)}) async-start(bf16[64,8,512]{2,1,0:T(8,128)(2,1)} %reduce_sum.94), calls=%async_computation.2 | async-start | bytes 1048576 | tf_op jit(solution)/shard_map/all_to_all | solution.py:240
  177.9 15.8 %all-to-all-done.2 = bf16[64,8,512]{2,1,0:T(8,128)(2,1)S(1)} async-done(((bf16[64,8,512]{2,1,0:T(8,128)(2,1)}), bf16[64,8,512]{2,1,0:T(8,128)(2,1)S(1)}, u32[]{:S(2)}, u32[]{:S(2)}) %all-to-all-start.2) | async-done | bytes 524320 | tf_op jit(solution)/shard_map/all_to_all | solution.py:240
  193.7 1.2 gather_fusion.2
  195.0 1.1 broadcast_in_dim.96
  196.1 4.2 %all-to-all-start.3 = ((bf16[4,128,2,512]{3,1,2,0:T(8,128)(2,1)}), bf16[4,128,2,512]{3,1,2,0:T(8,128)(2,1)}, u32[]{:S(2)}, u32[]{:S(2)}) async-start(bf16[4,128,2,512]{3,1,2,0:T(8,128)(2,1)} %broadcast_in_dim.96), calls=%async_computation.3 | async-start | bytes 2097152 | tf_op jit(solution)/shard_map/all_to_all | solution.py:95
  200.7 4.2 %fusion = bf16[1,2048,384]{2,1,0:T(8,128)(2,1)} fusion(bf16[512,384]{1,0:T(8,128)(2,1)S(1)} %copy-done.9, bf16[128,8,2048]{2,1,0:T(8,128)(2,1)} %all-gather.14.cloned.1.call-done), kind=kOutput, calls=%fused_computation.14 | convolution fusion | flops 806092800 | bytes 4063232 | tf_op jit(solution)/shard_map/rd,rf->df/dot_general | solution.py:228
  204.9 2.5 fusion.1
  207.3 2.2 fusion.2
  209.5 5.7 %all-to-all-done.3 = bf16[4,128,2,512]{3,1,2,0:T(8,128)(2,1)} async-done(((bf16[4,128,2,512]{3,1,2,0:T(8,128)(2,1)}), bf16[4,128,2,512]{3,1,2,0:T(8,128)(2,1)}, u32[]{:S(2)}, u32[]{:S(2)}) %all-to-all-start.3) | async-done | bytes 1048608 | tf_op jit(solution)/shard_map/all_to_all | solution.py:95
  215.2 1.5 convert_reduce_fusion
  218.6 0.9 multiply_reduce_fusion
  219.7 1.8 fusion.40
  222.3 2.8 all-gather.9
  225.8 9.4 %all-gather.10 = f32[4,129,128]{2,1,0:T(8,128)S(1)} all-gather(f32[1,129,128]{2,1,0:T(8,128)S(1)} %maximum_bitcast_fusion.2), channel_id=6, replica_groups=mesh['sp_0'=8,'sp_1'=4,'sp_2'=2,'tp'=4] {'sp_1'}, dimensions={0}, use_global_device_ids=true | all-gather | bytes 330240 | tf_op jit(solution)/shard_map/all_gather | solution.py:31
  235.4 23.1 %all-gather.11 = f32[8,129,128]{2,1,0:T(8,128)S(1)} all-gather(f32[1,129,128]{2,1,0:T(8,128)S(1)} %maximum_bitcast_fusion.3), channel_id=7, replica_groups=mesh['sp_0'=8,'sp_1'=4,'sp_2'=2,'tp'=4] {'sp_0'}, dimensions={0}, use_global_device_ids=true | all-gather | bytes 594432 | tf_op jit(solution)/shard_map/all_gather | solution.py:31
  264.2 0.9 fusion.96
  266.3 1.3 fusion.19
  268.5 0.7 convert_element_type.106
  269.3 0.7 convert_element_type.108
  272.0 1.1 reduce_window_sum.48
  273.1 16.8 %reduce-scatter.6.cloned.1.call-done = f32[64,256]{1,0:T(8,128)} async-done(((f32[256,256]{1,0:T(8,128)}), f32[64,256]{1,0:T(8,128)}) %reduce-scatter.6.cloned.1.call-update) | async-done | bytes 65552 | tf_op jit(solution)/shard_map/reduce_scatter | solution.py:104
  290.6 17.9 %reduce-scatter.8.cloned.1.call-done = f32[32,256]{1,0:T(8,128)} async-done(((f32[64,256]{1,0:T(8,128)}), f32[32,256]{1,0:T(8,128)}) %reduce-scatter.8.cloned.1.call-update) | async-done | bytes 32784 | tf_op jit(solution)/shard_map/reduce_scatter | solution.py:104
  (264 shorter events, 29.9 us)
Async XLA Ops:
  7.2 113.5 %copy-start = (bf16[1,2048,384]{2,1,0:T(8,128)(2,1)S(1)}, bf16[1,2048,384]{2,1,0:T(8,128)(2,1)}, u32[]{:S(2)}) copy-start(bf16[1,2048,384]{2,1,0:T(8,128)(2,1)} %param.23) | copy-start | bytes 4718596
  7.2 113.4 %all-gather.14.cloned.1.call-start = ((), (), s32[]{:S(2)}) async-start(), calls=%async_computation.7 | async-start | bytes 5242880 | tf_op jit(solution)/shard_map/all_gather | solution.py:71
  12.5 3.8 %copy-start.25 = (f32[128,2]{0,1:T(2,128)S(1)}, f32[128,2]{0,1:T(2,128)}, u32[]{:S(2)}) copy-start(f32[128,2]{0,1:T(2,128)} %param.21) | copy-start | bytes 3076
  12.5 6.8 %copy-start.1 = (bf16[128,2048]{1,0:T(8,128)(2,1)S(1)}, bf16[128,2048]{1,0:T(8,128)(2,1)}, u32[]{:S(2)}) copy-start(bf16[128,2048]{1,0:T(8,128)(2,1)} %param.18) | copy-start | bytes 1572868
  17.8 3.6 %copy-start.34 = (s32[256,1]{0,1:T(1,128)}, s32[256,1]{0,1:T(1,128)S(1)}, u32[]{:S(2)}) copy-start(s32[256,1]{0,1:T(1,128)S(1)} %compare_select_fusion) | copy-start | bytes 3076
  19.5 1.9 copy-start.26
  19.5 1.9 copy-start.12
  71.9 1.3 copy-start.16
  71.9 1.4 copy-start.19
  73.8 15.2 %copy-start.37 = (f32[1,128]{1,0:T(1,128)}, f32[1,128]{1,0:T(1,128)S(1)}, u32[]{:S(2)}) copy-start(f32[1,128]{1,0:T(1,128)S(1)} %exp.66) | copy-start | bytes 1540
  75.0 101.0 %copy-start.5 = (f32[2,2,64,128]{3,2,1,0:T(8,128)}, f32[2,2,64,128]{3,2,1,0:T(8,128)S(1)}, u32[]{:S(2)}) copy-start(f32[2,2,64,128]{3,2,1,0:T(8,128)S(1)} %get-tuple-element.140) | copy-start | bytes 393220
  89.0 52.8 %copy-start.30 = (f32[2,64]{1,0:T(2,128)}, f32[2,64]{1,0:T(2,128)S(1)}, u32[]{:S(2)}) copy-start(f32[2,64]{1,0:T(2,128)S(1)} %squeeze.170) | copy-start | bytes 1540
  89.1 52.8 %copy-start.31 = (f32[2,64]{1,0:T(2,128)}, f32[2,64]{1,0:T(2,128)S(1)}, u32[]{:S(2)}) copy-start(f32[2,64]{1,0:T(2,128)S(1)} %squeeze.169) | copy-start | bytes 1540
  89.2 52.7 %copy-start.32 = (f32[2,64]{1,0:T(2,128)}, f32[2,64]{1,0:T(2,128)S(1)}, u32[]{:S(2)}) copy-start(f32[2,64]{1,0:T(2,128)S(1)} %squeeze.168) | copy-start | bytes 1540
  90.0 51.9 %copy-start.33 = (f32[2,64]{1,0:T(2,128)}, f32[2,64]{1,0:T(2,128)S(1)}, u32[]{:S(2)}) copy-start(f32[2,64]{1,0:T(2,128)S(1)} %squeeze.172) | copy-start | bytes 1540
  120.6 3.0 copy-start.4
  120.6 3.3 %copy-start.49 = (bf16[128,8,2048]{2,1,0:T(8,128)(2,1)S(1)}, bf16[128,8,2048]{2,1,0:T(8,128)(2,1)}, u32[]{:S(2)}) copy-start(bf16[128,8,2048]{2,1,0:T(8,128)(2,1)} %all-gather.14.cloned.1.call-done) | copy-start | bytes 12582916
  123.9 1.7 copy-start.51
  125.6 1.5 copy-start.54
  131.2 9.8 %copy-start.20 = (bf16[128,128]{1,0:T(8,128)(2,1)S(1)}, bf16[128,128]{1,0:T(8,128)(2,1)}, u32[]{:S(2)}) copy-start(bf16[128,128]{1,0:T(8,128)(2,1)} %param.27) | copy-start | bytes 98308
  131.2 10.7 %copy-start.39 = (f32[2,64]{1,0:T(2,128)S(1)}, f32[2,64]{1,0:T(2,128)}, u32[]{:S(2)}) copy-start(f32[2,64]{1,0:T(2,128)} %squeeze.167) | copy-start | bytes 1540
  131.2 10.7 %copy-start.40 = (f32[2,64]{1,0:T(2,128)S(1)}, f32[2,64]{1,0:T(2,128)}, u32[]{:S(2)}) copy-start(f32[2,64]{1,0:T(2,128)} %squeeze.171) | copy-start | bytes 1540
  131.2 30.2 %all-to-all-start.1 = ((bf16[4,64,8,512]{3,2,1,0:T(8,128)(2,1)}), bf16[4,64,8,512]{3,2,1,0:T(8,128)(2,1)}, u32[]{:S(2)}, u32[]{:S(2)}) async-start(bf16[4,64,8,512]{3,2,1,0:T(8,128)(2,1)} %bitcast.286), calls=%async_computation.1 | async-start | bytes 4194304 | tf_op jit(solution)/shard_map/all_to_all | solution.py:83
  141.3 35.2 %copy-start.13 = (pred[64,64]{1,0:T(8,128)(4,1)}, pred[64,64]{1,0:T(8,128)(4,1)S(1)}, u32[]{:S(2)}) copy-start(pred[64,64]{1,0:T(8,128)(4,1)S(1)} %iota_compare_fusion.2) | copy-start | bytes 12292
  142.0 34.0 %copy-start.35 = (s32[256,1]{0,1:T(1,128)S(1)}, s32[256,1]{0,1:T(1,128)}, u32[]{:S(2)}) copy-start(s32[256,1]{0,1:T(1,128)} %copy-done.34) | copy-start | bytes 3076
  142.0 34.0 %copy-start.23 = (f32[2,2,64]{2,1,0:T(2,128)S(1)}, f32[2,2,64]{2,1,0:T(2,128)}, u32[]{:S(2)}) copy-start(f32[2,2,64]{2,1,0:T(2,128)} %get-tuple-element.289) | copy-start | bytes 3076
  164.3 29.4 %all-to-all-start.2 = ((bf16[64,8,512]{2,1,0:T(8,128)(2,1)}), bf16[64,8,512]{2,1,0:T(8,128)(2,1)S(1)}, u32[]{:S(2)}, u32[]{:S(2)}) async-start(bf16[64,8,512]{2,1,0:T(8,128)(2,1)} %reduce_sum.94), calls=%async_computation.2 | async-start | bytes 1048576 | tf_op jit(solution)/shard_map/all_to_all | solution.py:240
  195.0 5.7 %copy-start.9 = (bf16[512,384]{1,0:T(8,128)(2,1)S(1)}, bf16[512,384]{1,0:T(8,128)(2,1)}, u32[]{:S(2)}) copy-start(bf16[512,384]{1,0:T(8,128)(2,1)} %copy-done.8) | copy-start | bytes 1179652
  196.1 19.1 %all-to-all-start.3 = ((bf16[4,128,2,512]{3,1,2,0:T(8,128)(2,1)}), bf16[4,128,2,512]{3,1,2,0:T(8,128)(2,1)}, u32[]{:S(2)}, u32[]{:S(2)}) async-start(bf16[4,128,2,512]{3,1,2,0:T(8,128)(2,1)} %broadcast_in_dim.96), calls=%async_computation.3 | async-start | bytes 2097152 | tf_op jit(solution)/shard_map/all_to_all | solution.py:95
  200.4 4.5 %copy-start.11 = (bf16[512,384]{1,0:T(8,128)(2,1)S(1)}, bf16[512,384]{1,0:T(8,128)(2,1)}, u32[]{:S(2)}) copy-start(bf16[512,384]{1,0:T(8,128)(2,1)} %copy-done.10) | copy-start | bytes 1179652
  200.4 67.6 %reduce-scatter.4.cloned.1.call-start = ((), (), s32[]{:S(2)}) async-start(), calls=%async_computation.8 | async-start | bytes 2359296 | tf_op jit(solution)/shard_map/reduce_scatter | solution.py:104
  200.7 4.2 %copy-start.50 = (bf16[128,8,2048]{2,1,0:T(8,128)(2,1)S(1)}, bf16[128,8,2048]{2,1,0:T(8,128)(2,1)}, u32[]{:S(2)}) copy-start(bf16[128,8,2048]{2,1,0:T(8,128)(2,1)} %all-gather.14.cloned.1.call-done) | copy-start | bytes 12582916
  204.9 2.5 copy-start.53
  204.9 2.5 copy-start.55
  209.5 7.3 %copy-start.2 = (bf16[128,2048]{1,0:T(8,128)(2,1)S(1)}, bf16[128,2048]{1,0:T(8,128)(2,1)}, u32[]{:S(2)}) copy-start(bf16[128,2048]{1,0:T(8,128)(2,1)} %param.18) | copy-start | bytes 1572868
  209.5 7.3 %copy-start.27 = (f32[128]{0:T(128)S(1)}, f32[128]{0:T(128)}, u32[]{:S(2)}) copy-start(f32[128]{0:T(128)} %copy-done.26) | copy-start | bytes 1540
  216.9 1.3 copy-start.7
  218.2 1.3 copy-start.21
  221.6 68.3 %reduce-scatter.6.cloned.1.call-start = ((), (), s32[]{:S(2)}) async-start(), calls=%async_computation.9 | async-start | bytes 327680 | tf_op jit(solution)/shard_map/reduce_scatter | solution.py:104
  222.0 43.1 %copy-start.14 = (pred[64,64]{1,0:T(8,128)(4,1)S(1)}, pred[64,64]{1,0:T(8,128)(4,1)}, u32[]{:S(2)}) copy-start(pred[64,64]{1,0:T(8,128)(4,1)} %copy-done.13) | copy-start | bytes 12292
  225.1 40.3 %copy-start.36 = (f32[2,64]{1,0:T(2,128)S(1)}, f32[2,64]{1,0:T(2,128)}, u32[]{:S(2)}) copy-start(f32[2,64]{1,0:T(2,128)} %fusion.88) | copy-start | bytes 1540
  235.3 30.6 %copy-start.18 = (f32[2,2,64]{2,1,0:T(2,128)S(1)}, f32[2,2,64]{2,1,0:T(2,128)}, u32[]{:S(2)}) copy-start(f32[2,2,64]{2,1,0:T(2,128)} %copy-done.17) | copy-start | bytes 3076
  235.3 30.6 %copy-start.22 = (f32[2,2,64]{2,1,0:T(2,128)S(1)}, f32[2,2,64]{2,1,0:T(2,128)}, u32[]{:S(2)}) copy-start(f32[2,2,64]{2,1,0:T(2,128)} %get-tuple-element.291) | copy-start | bytes 3076
  258.4 7.8 %copy-start.24 = (f32[2,2,64]{2,1,0:T(2,128)S(1)}, f32[2,2,64]{2,1,0:T(2,128)}, u32[]{:S(2)}) copy-start(f32[2,2,64]{2,1,0:T(2,128)} %get-tuple-element.289) | copy-start | bytes 3076
  264.1 1.3 copy-start.46
  264.1 1.3 copy-start.47
  264.1 1.3 copy-start.48
  268.0 40.4 %reduce-scatter.8.cloned.1.call-start = ((), (), s32[]{:S(2)}) async-start(), calls=%async_computation.10 | async-start | bytes 98304 | tf_op jit(solution)/shard_map/reduce_scatter | solution.py:104
  (15 other events, 17.6 us)
Sparse Core Ops, SparseCore 0:
  73.1 47.4 all-gather.13
  221.7 34.6 reduce-scatter.3
  268.1 21.7 reduce-scatter.5
  292.8 15.6 reduce-scatter.7
where the time goes:
time: 316 us; the launch traced here: 315 us
  blocking collectives  112 us (35%)
  waiting for transfers between devices  82.8 us (26%)
  local copies, waits for them, and re-layouts  43.1 us (14%)
  matrix products  24.4 us (8%)
  starting transfers between devices  20.9 us (7%)
  other arithmetic  16.8 us (5%)
  between operations  15 us (5%)
    all_gather x6, blocking collectives, collected_together(): both, at, found = (lax.all_gather(jnp.concatenate(lines), axis), 0, {})  70.6 us
    all_to_all x1, blocking collectives, side_by_side(): lax.all_to_all(both, axis, split_axis=split_dim, concat_axis=concat_dim,...  41.1 us
    reduce_scatter x3, waiting for transfers between devices, own_rows(): so_far = lax.psum_scatter(so_far, axis, scatter_dimension=0, tiled=True)  34.7 us
    all_to_all x1, waiting for transfers between devices, sent_and_summed(): lax.all_to_all(split_up(array, dim, length), axis, 0, 0, tiled=True)  18.3 us
    all_to_all x1, waiting for transfers between devices, body(): lax.all_to_all(summed, SP, split_axis=0, concat_axis=0, tiled=True)  15.8 us
    all_to_all x1, starting transfers between devices, body(): lax.all_to_all(summed, SP, split_axis=0, concat_axis=0, tiled=True)  11.7 us
    all_gather x1, waiting for transfers between devices, side_by_side_2(): result = lax.all_gather(both, axis, axis=dim, tiled=True)  8.27 us
    mul x3, local copies, waits for them, and re-layouts, body(): route_weight[:, :, None] * cot_f[:, None, :]  7.3 us
  transfers between devices with their start and end apart: 7, of which 6 were waited for; matrix products, arithmetic and copies ran while one was open for 12% of the time, Pallas kernels for 0%

commit v1 on v0

v1 whole, which is shorter than its diff:
```python
import jax
import jax.numpy as jnp
from jax import lax
from jax.experimental import pallas as pl
from jax.experimental.pallas import tpu as pltpu
from jax.sharding import Mesh
from jax.sharding import PartitionSpec as P

KEY_DIM = 64
VAL_DIM = 128
BLOCK = 64
SP = ("sp_0", "sp_1", "sp_2")
GROUP = ("sp_1", "sp_2")
N_TP = 4
N_Z = 8
HIGH = lax.Precision.HIGHEST
EPS = 1e-06
F32 = jnp.float32
BF16 = jnp.bfloat16


def exchange(array, axis):
    return lax.all_to_all(array, axis, split_axis=0, concat_axis=0, tiled=True)


def shifted(array, by):
    return lax.ppermute(array, "tp", [((k + by) % N_TP, k) for k in range(N_TP)])


def whole():
    return pl.BlockSpec(memory_space=pltpu.VMEM)


def scalars():
    return pl.BlockSpec(memory_space=pltpu.SMEM)


def run(kernel, name, outs, numbers, *arrays):
    numbers = jnp.stack(numbers) if numbers else jnp.zeros((1,), jnp.int32)
    return pl.pallas_call(
        kernel,
        out_shape=tuple(jax.ShapeDtypeStruct(shape, dtype) for shape, dtype in outs),
        in_specs=[scalars()] + [whole()] * len(arrays),
        out_specs=tuple(whole() for _ in outs),
        name=name,
    )(numbers, *arrays)


def iota(shape, dim):
    return lax.broadcasted_iota(jnp.int32, shape, dim)


def exact(a, b, dims):
    return lax.dot_general(a, b, (dims, ((), ())), precision=HIGH, preferred_element_type=F32)


NN = ((1,), (0,))
NT = ((1,), (1,))
TN = ((0,), (0,))


def paired(a, b, dims):
    return lax.dot_general(a, b, (dims, ((), ())), preferred_element_type=F32)


def dispatch_kernel(rank_ref, hidden_ref, gain_ref, ids_ref, logits_ref, cot_ref, send_ref, place_ref):
    rank = rank_ref[0]
    tok, width = hidden_ref.shape
    quarter = width // 4
    state = hidden_ref[...].astype(F32)
    scale = lax.rsqrt(jnp.mean(state * state, axis=-1, keepdims=True) + EPS)
    normed = ((state * scale) * gain_ref[...]).astype(BF16)
    logits = logits_ref[...]
    l0, l1 = logits[:, 0:1], logits[:, 1:2]
    top = jnp.maximum(l0, l1)
    e0, e1 = jnp.exp(l0 - top), jnp.exp(l1 - top)
    total = e0 + e1
    cot = cot_ref[...].astype(F32)
    grads = [((e / total) * cot).astype(BF16) for e in (e0, e1)]
    rows_all = send_ref.shape[0]
    experts = rows_all // 8
    ids = ids_ref[...]
    eye = iota((experts, tok), 0)
    hot = [(eye == ids[r : r + 1, :]).astype(F32) for r in range(2)]
    earlier = (iota((tok, tok), 0) < iota((tok, tok), 1)).astype(F32)
    before = paired(hot[0] + hot[1], earlier, NN)
    rows = iota((rows_all, tok), 0)
    kept, places = [], []
    for r in range(2):
        slot = jnp.sum(before * hot[r], axis=0, keepdims=True).astype(jnp.int32)
        block = slot >> 1
        first = 8 * ids[r : r + 1, :] + (slot & 1)
        kept.append(jnp.where(block == rank, first, -8))
        places.append(first + 2 * ((block - rank) & 3))
    place_ref[...] = jnp.concatenate(places, axis=0)
    total_in, total_grad = None, None
    for h in range(4):
        pick = [(rows == kept[r] + 2 * h).astype(F32) for r in range(2)]
        lanes = slice(h * quarter, (h + 1) * quarter)
        term = paired((pick[0] + pick[1]).astype(BF16), normed[:, lanes], NN)
        total_in = term if total_in is None else total_in + term
        term = paired(pick[0].astype(BF16), grads[0][:, lanes], NN)
        term = term + paired(pick[1].astype(BF16), grads[1][:, lanes], NN)
        total_grad = term if total_grad is None else total_grad + term
    send_ref[:, :quarter] = total_in.astype(BF16)
    send_ref[:, quarter:] = total_grad.astype(BF16)


def unpack_kernel(_, got_ref, out_ref):
    got = got_ref[...]
    rows, width = out_ref.shape
    quarter = width // 8
    line = iota((rows, got.shape[0]), 0)
    col = iota((rows, got.shape[0]), 1)
    for h in range(4):
        pick = (col == 8 * (line >> 1) + 2 * h + (line & 1)).astype(F32).astype(BF16)
        both = paired(pick, got, NN).astype(BF16)
        out_ref[:, h * quarter : (h + 1) * quarter] = both[:, :quarter]
        out_ref[:, (4 + h) * quarter : (5 + h) * quarter] = both[:, quarter:]


def combine_kernel(_, own_ref, one_ref, two_ref, three_ref, out_ref):
    rows = own_ref.shape[0] // 4
    line = iota((4 * rows, rows), 0)
    col = iota((4 * rows, rows), 1)
    total = None
    for k in range(4):
        acc = own_ref[k * rows : (k + 1) * rows].astype(F32)
        for by, ref in ((1, one_ref), (2, two_ref), (3, three_ref)):
            m = (k + by) % 4
            acc = acc + ref[m * rows : (m + 1) * rows].astype(F32)
        spread = (line == 8 * (col >> 1) + 2 * k + (col & 1)).astype(F32).astype(BF16)
        term = paired(spread, acc.astype(BF16), NN)
        total = term if total is None else total + term
    out_ref[...] = total.astype(BF16)


def pick_kernel(_, returned_ref, place_ref, out_ref):
    tok = out_ref.shape[0]
    slots = iota((returned_ref.shape[0], tok), 0)
    here = ((slots == place_ref[0:1, :]) | (slots == place_ref[1:2, :])).astype(F32).astype(BF16)
    out_ref[...] = paired(here, returned_ref[...], TN).astype(BF16)


def by_head(x):
    half = x.shape[0] // 2
    return jnp.concatenate([x[:half, :VAL_DIM], x[half:, VAL_DIM:]], axis=0)


def spread_heads(x):
    half = x.shape[0] // 2
    zero = jnp.zeros((half, VAL_DIM), F32)
    return jnp.concatenate(
        [jnp.concatenate([x[:half], zero], axis=1), jnp.concatenate([zero, x[half:]], axis=1)], axis=0
    )


def same_block(t, s):
    return (t // BLOCK) == (s // BLOCK)


def mids(cum):
    tok, keys = cum.shape
    row = iota((tok, keys), 0)
    mid = jnp.where(row < BLOCK, cum[BLOCK // 2 : BLOCK // 2 + 1], cum[BLOCK + BLOCK // 2 : BLOCK + BLOCK // 2 + 1])
    last = jnp.where(row < BLOCK, cum[BLOCK - 1 : BLOCK], cum[2 * BLOCK - 1 : 2 * BLOCK])
    return mid, last


def pack_state(out_ref, state, log_row):
    keys = state.shape[0]
    high = log_row.astype(BF16).astype(F32)
    rest = log_row - high
    middle = rest.astype(BF16).astype(F32)
    low = rest - middle
    line = iota((16, state.shape[1]), 0)
    extra = jnp.where(line == 0, high, jnp.where(line == 1, middle, jnp.where(line == 2, low, 0.0)))
    block = state.astype(BF16)
    extra = extra.astype(BF16)
    for k in range(out_ref.shape[0]):
        out_ref[k, :keys, :] = block
        out_ref[k, keys:, :] = extra


def local_kernel(_, key_ref, value_ref, log_ref, pack_ref, cum_ref, cols_ref, first_ref, end_ref):
    tok, keys = key_ref.shape
    logs = log_ref[...]
    t, s = iota((tok, tok), 0), iota((tok, tok), 1)
    lower = ((t >= s) & same_block(t, s)).astype(F32)
    cum = exact(lower, logs, NN)
    cum_ref[...] = cum
    _, last = mids(cum)
    chosen = ((t // BLOCK) == s).astype(F32)
    cols = exact(logs, chosen, TN)
    cols_ref[...] = cols
    key_end = key_ref[...].astype(F32) * jnp.exp(last - cum)
    value = value_ref[...].astype(F32)
    first = by_head(exact(key_end[:BLOCK], value[:BLOCK], TN))
    second = by_head(exact(key_end[BLOCK:], value[BLOCK:], TN))
    end = jnp.exp(cols[:, 1:2]) * first + second
    first_ref[...] = first
    end_ref[...] = end
    pack_state(pack_ref, end, cum[BLOCK - 1 : BLOCK] + cum[2 * BLOCK - 1 : 2 * BLOCK])


def log_rows(got_ref, keys):
    return jnp.concatenate(
        [
            jnp.sum(got_ref[k, keys:, :].astype(F32), axis=0, keepdims=True)
            for k in range(got_ref.shape[0])
        ],
        axis=0,
    )


def walked(term_of, decays, position, length, reverse):
    carried = jnp.zeros((decays.shape[0], VAL_DIM), F32)
    here = carried
    for k in reversed(range(length)) if reverse else range(length):
        here = jnp.where(position == k, carried, here)
        carried = decays[:, k : k + 1] * carried + term_of(k)
    return here, carried


def group_kernel(spot_ref, got_ref, pack_ref, before_ref, cols_ref):
    length, _, keys = got_ref.shape
    rows = log_rows(got_ref, keys)
    cols = jnp.transpose(rows)
    cols_ref[...] = cols
    here, carried = walked(
        lambda k: got_ref[k, :keys, :].astype(F32), jnp.exp(cols), spot_ref[0], length, False
    )
    before_ref[...] = here
    pack_state(pack_ref, carried, jnp.sum(rows, axis=0, keepdims=True))


def forward_kernel(
    spot_ref,
    got_ref,
    before_ref,
    group_ref,
    query_ref,
    key_ref,
    value_ref,
    cum_ref,
    cols_ref,
    first_ref,
    out_ref,
    state_ref,
    zcols_ref,
):
    length, _, keys = got_ref.shape
    cols = jnp.transpose(log_rows(got_ref, keys))
    zcols_ref[...] = cols
    before_z, _ = walked(
        lambda k: got_ref[k, :keys, :].astype(F32), jnp.exp(cols), spot_ref[1], length, False
    )
    group = group_ref[...]
    lead = jnp.sum(jnp.where(iota(group.shape, 1) < spot_ref[0], group, 0.0), axis=1, keepdims=True)
    state = before_ref[...] + jnp.exp(lead) * before_z
    state_ref[...] = state
    cum = cum_ref[...]
    tok = cum.shape[0]
    mid, _ = mids(cum)
    query = query_ref[...].astype(F32)
    query_in = query * jnp.exp(cum - mid)
    key_in = key_ref[...].astype(F32) * jnp.exp(mid - cum)
    value = value_ref[...].astype(F32)
    start = query * jnp.exp(cum)
    t, s = iota((tok, tok), 0), iota((tok, tok), 1)
    causal = (t >= s) & same_block(t, s)
    lane = iota((tok, keys), 1) // KEY_DIM
    later = first_ref[...] + jnp.exp(cols_ref[:, 0:1]) * state
    outside = jnp.concatenate(
        [exact(start[:BLOCK], spread_heads(state), NN), exact(start[BLOCK:], spread_heads(later), NN)],
        axis=0,
    )
    for h in range(2):
        lanes = slice(h * VAL_DIM, (h + 1) * VAL_DIM)
        scores = exact(jnp.where(lane == h, query_in, 0.0), key_in, NT)
        scores = jnp.where(causal, scores, 0.0)
        out_ref[:, lanes] = exact(scores, value[:, lanes], NN) + outside[:, lanes]


def head_norm(head_out, gain):
    normed, scale = [], []
    for h in range(2):
        x = head_out[:, h * VAL_DIM : (h + 1) * VAL_DIM]
        r = lax.rsqrt(jnp.mean(x * x, axis=-1, keepdims=True) + EPS)
        scale.append(r)
        normed.append(x * r)
    return normed, scale


def mixer_kernel(
    rank_ref,
    own_ref,
    one_ref,
    two_ref,
    three_ref,
    hidden_ref,
    cot_ref,
    gain_ref,
    w_out_ref,
    head_ref,
    head_gain_ref,
    query_ref,
    cum_ref,
    cols_ref,
    pack_ref,
    grad_ref,
    adj_ref,
    mixed_ref,
):
    rank = rank_ref[0]
    tok, width = hidden_ref.shape
    part = width // 4
    state = hidden_ref[...].astype(F32)
    scale = lax.rsqrt(jnp.mean(state * state, axis=-1, keepdims=True) + EPS)
    parts = (own_ref, one_ref, two_ref, three_ref)
    inner = jnp.zeros((tok, 1), F32)
    for k in range(4):
        at = pl.multiple_of(((rank + k) & 3) * part, part)
        unit = hidden_ref[:, pl.ds(at, part)].astype(F32) * scale
        u = parts[k][...].astype(F32) * gain_ref[:, pl.ds(at, part)]
        inner = inner + jnp.sum(u * unit, axis=-1, keepdims=True)
    inner = inner / width
    grad_mix = None
    for k in range(4):
        at = pl.multiple_of(((rank + k) & 3) * part, part)
        unit = hidden_ref[:, pl.ds(at, part)].astype(F32) * scale
        u = parts[k][...].astype(F32) * gain_ref[:, pl.ds(at, part)]
        mixed = (cot_ref[:, pl.ds(at, part)].astype(F32) + scale * (u - unit * inner)).astype(BF16)
        mixed_ref[:, pl.ds(at, part)] = mixed
        term = paired(mixed, w_out_ref[pl.ds(at, part), :], NN)
        grad_mix = term if grad_mix is None else grad_mix + term
    grad_mix = grad_mix.astype(BF16).astype(F32)
    head_gain = head_gain_ref[...]
    normed, head_scale = head_norm(head_ref[...], head_gain)
    out = []
    for h in range(2):
        lanes = slice(h * VAL_DIM, (h + 1) * VAL_DIM)
        u = grad_mix[:, lanes] * head_gain[:, lanes]
        n = normed[h]
        out.append(head_scale[h] * (u - n * jnp.mean(u * n, axis=-1, keepdims=True)))
    grad = jnp.concatenate(out, axis=1)
    grad_ref[...] = grad
    start = query_ref[...].astype(F32) * jnp.exp(cum_ref[...])
    early = by_head(exact(start[:BLOCK], grad[:BLOCK], TN))
    late = by_head(exact(start[BLOCK:], grad[BLOCK:], TN))
    adj_ref[...] = late
    local = (jnp.exp(cols_ref[:, 0:1]) * late + early).astype(BF16)
    half = local.shape[0] // 2
    n_g, rows, _ = pack_ref.shape
    n_z = N_Z
    each = (rows - half) // n_z
    state_rows = jnp.concatenate([local[:half], local[half:]], axis=1)
    mixed_out = jnp.concatenate(
        [normed[h] * head_gain[:, h * VAL_DIM : (h + 1) * VAL_DIM] for h in range(2)], axis=1
    ).astype(BF16)
    out_part = paired(mixed_ref[...], mixed_out, TN).astype(BF16)

    for q in range(n_g):
        for z in range(n_z):
            at = (z * n_g + q) * each
            pack_ref[q, z * each : (z + 1) * each, :] = out_part[at : at + each]
        pack_ref[q, n_z * each :, :] = state_rows


def states_of(rows):
    return jnp.concatenate([rows[:, :VAL_DIM], rows[:, VAL_DIM:]], axis=0).astype(F32)


def behind_kernel(spot_ref, got_ref, cols_ref, pack_ref, after_ref):
    length, rows, _ = got_ref.shape
    n_z, each = pack_ref.shape[0], pack_ref.shape[1]
    half = after_ref.shape[0] // 2
    each = each - half
    total = got_ref[0, : rows - half, :].astype(F32)
    for k in range(1, length):
        total = total + got_ref[k, : rows - half, :].astype(F32)
    total = total.astype(BF16)
    here, carried = walked(
        lambda k: states_of(got_ref[k, rows - half :, :]), jnp.exp(cols_ref[...]), spot_ref[0], length, True
    )
    after_ref[...] = here
    carried = carried.astype(BF16)
    state_rows = jnp.concatenate([carried[:half], carried[half:]], axis=1)
    for z in range(n_z):
        pack_ref[z, :each, :] = total[z * each : (z + 1) * each]
        pack_ref[z, each:, :] = state_rows


def inner_kernel(
    _,
    query_ref,
    key_ref,
    value_ref,
    cum_ref,
    cols_ref,
    first_ref,
    state_ref,
    grad_ref,
    dq_ref,
    dk_ref,
    dv_ref,
    dlog_ref,
):
    cum = cum_ref[...]
    tok, keys = cum.shape
    mid, _ = mids(cum)
    query, key = query_ref[...].astype(F32), key_ref[...].astype(F32)
    rise, fall = jnp.exp(cum - mid), jnp.exp(mid - cum)
    query_in, key_in = query * rise, key * fall
    value, grad = value_ref[...].astype(F32), grad_ref[...]
    t, s = iota((tok, tok), 0), iota((tok, tok), 1)
    causal = (t >= s) & same_block(t, s)
    lane = iota((tok, keys), 1) // KEY_DIM
    state = state_ref[...]
    later = first_ref[...] + jnp.exp(cols_ref[:, 0:1]) * state
    outside = jnp.concatenate(
        [exact(grad[:BLOCK], spread_heads(state), NT), exact(grad[BLOCK:], spread_heads(later), NT)],
        axis=0,
    )
    dq = jnp.zeros((tok, keys), F32)
    dk = jnp.zeros((tok, keys), F32)
    for h in range(2):
        lanes = slice(h * VAL_DIM, (h + 1) * VAL_DIM)
        mine = lane == h
        dots = jnp.where(causal, exact(grad[:, lanes], value[:, lanes], NT), 0.0)
        scores = jnp.where(causal, exact(jnp.where(mine, query_in, 0.0), key_in, NT), 0.0)
        dq = jnp.where(mine, exact(dots, key_in, NN), dq)
        dk = jnp.where(mine, exact(dots, query_in, TN), dk)
        dv_ref[:, lanes] = exact(scores, grad[:, lanes], TN)
    dq = rise * dq + jnp.exp(cum) * outside
    dk = fall * dk
    dq_ref[...] = dq.astype(BF16)
    dk_ref[...] = dk
    dlog_ref[...] = query * dq - key * dk


def final_kernel(
    spot_ref,
    got_ref,
    zcols_ref,
    group_ref,
    after_ref,
    key_ref,
    value_ref,
    cum_ref,
    cols_ref,
    adj_ref,
    state_ref,
    end_ref,
    dk_in_ref,
    dv_in_ref,
    dlog_in_ref,
    dw_ref,
    dk_ref,
    dv_ref,
    dlog_ref,
):
    length, rows, _ = got_ref.shape
    keys = cum_ref.shape[1]
    half = keys // 2
    each = rows - half
    total = got_ref[0, :each, :].astype(F32)
    for k in range(1, length):
        total = total + got_ref[k, :each, :].astype(F32)
    dw_ref[...] = total
    after_z, _ = walked(
        lambda k: states_of(got_ref[k, each:, :]), jnp.exp(zcols_ref[...]), spot_ref[1], length, True
    )
    group = group_ref[...]
    tail = jnp.sum(jnp.where(iota(group.shape, 1) > spot_ref[0], group, 0.0), axis=1, keepdims=True)
    end = after_ref[...] + jnp.exp(tail) * after_z
    cols = cols_ref[...]
    middle = adj_ref[...] + jnp.exp(cols[:, 1:2]) * end
    early, late = spread_heads(middle), spread_heads(end)
    cum = cum_ref[...]
    tok = cum.shape[0]
    _, last = mids(cum)
    fade = jnp.exp(last - cum)
    key = key_ref[...].astype(F32)
    key_end = key * fade
    value = value_ref[...].astype(F32)
    dv_ref[:BLOCK, :] = (dv_in_ref[:BLOCK, :] + exact(key_end[:BLOCK], early, NN)).astype(BF16)
    dv_ref[BLOCK:, :] = (dv_in_ref[BLOCK:, :] + exact(key_end[BLOCK:], late, NN)).astype(BF16)
    more = fade * jnp.concatenate(
        [exact(value[:BLOCK], early, NT), exact(value[BLOCK:], late, NT)], axis=0
    )
    dk_ref[...] = (dk_in_ref[...] + more).astype(BF16)
    terms = dlog_in_ref[...] - key * more
    t, s = iota((tok, tok), 0), iota((tok, tok), 1)
    upper = (t <= s).astype(F32)
    end_state = jnp.exp(cols[:, 0:1] + cols[:, 1:2]) * state_ref[...] + end_ref[...]
    ones = jnp.ones((tok, VAL_DIM), F32)
    dlog_ref[...] = exact(upper, terms, NN) + exact(ones, end * end_state, NT)


def body(
    hidden_state,
    norm_gain,
    route_ids,
    route_logits,
    cotangent,
    w_gate,
    w_up,
    w_down,
    w_out,
    query_rows,
    key_rows,
    value_rows,
    log_decay,
    head_gain,
):
    tok_count, model_width = hidden_state.shape
    rank = lax.axis_index("tp")
    spot_z = lax.axis_index("sp_0")
    spot_g = lax.axis_index(GROUP)
    n_z, n_g = lax.axis_size("sp_0"), lax.axis_size(GROUP)
    experts = n_z * n_g
    part = model_width // N_TP
    keys = key_rows.shape[1]
    values = value_rows.shape[1]
    gain_row = norm_gain.reshape(1, model_width)
    head_gain_row = head_gain.reshape(1, values)
    spots = [spot_g, spot_z]

    send, place = run(
        dispatch_kernel,
        "dispatch",
        [((8 * experts, 2 * part), BF16), ((2, tok_count), jnp.int32)],
        [rank],
        hidden_state,
        gain_row,
        route_ids.T,
        route_logits,
        cotangent,
    )
    got = exchange(send.reshape(experts, 8, 2 * part), SP).reshape(8 * experts, 2 * part)
    (mine,) = run(unpack_kernel, "unpack", [((2 * experts, 2 * model_width), BF16)], [], got)

    square = ((keys, VAL_DIM), F32)
    packed, cum, cols, first, end = run(
        local_kernel,
        "local",
        [((n_g, keys + 16, VAL_DIM), BF16), ((tok_count, keys), F32), ((keys, tok_count), F32), square, square],
        [],
        key_rows,
        value_rows,
        log_decay,
    )
    got = exchange(packed, GROUP)
    packed, before_g, group_cols = run(
        group_kernel,
        "group",
        [((n_z, keys + 16, VAL_DIM), BF16), square, ((keys, n_g), F32)],
        spots,
        got,
    )
    got = exchange(packed, "sp_0")
    head_out, state_in, z_cols = run(
        forward_kernel,
        "forward",
        [((tok_count, values), F32), square, ((keys, n_z), F32)],
        spots,
        got,
        before_g,
        group_cols,
        query_rows,
        key_rows,
        value_rows,
        cum,
        cols,
        first,
    )

    left = shifted(mine, -1)
    right = shifted(mine, 1)
    far_in = shifted(left[:, :model_width], -1)
    far_grad = shifted(right[:, model_width:], 1)
    rows_in = jnp.concatenate(
        [mine[:, :model_width], right[:, :model_width], far_in, left[:, :model_width]]
    )
    rows_grad = jnp.concatenate(
        [mine[:, model_width:], right[:, model_width:], far_grad, left[:, model_width:]]
    )
    gate_w, up_w, down_w = w_gate[0], w_up[0], w_down[0]
    gate_pre = jnp.dot(rows_in, gate_w, preferred_element_type=F32)
    up_pre = jnp.dot(rows_in, up_w, preferred_element_type=F32)
    gate_sig = jax.nn.sigmoid(gate_pre)
    silu_gate = gate_pre * gate_sig
    hidden_units = (silu_gate * up_pre).astype(BF16)
    grad_hidden = jnp.einsum("rd,fd->rf", rows_grad, down_w, preferred_element_type=F32)
    grad_gate_pre = (grad_hidden * up_pre * gate_sig * (1.0 + gate_pre * (1.0 - gate_sig))).astype(BF16)
    grad_up_pre = (grad_hidden * silu_gate).astype(BF16)

    def features_of(by):
        start = ((rank + by) & 3) * part
        gate_part = lax.dynamic_slice_in_dim(gate_w, start, part, 0)
        up_part = lax.dynamic_slice_in_dim(up_w, start, part, 0)
        rows = jnp.einsum("rf,df->rd", grad_gate_pre, gate_part, preferred_element_type=F32)
        rows = rows + jnp.einsum("rf,df->rd", grad_up_pre, up_part, preferred_element_type=F32)
        return rows.astype(BF16)

    two = shifted(features_of(2), -2)
    one = shifted(features_of(1), -1)
    three = shifted(features_of(3), -3)
    own = features_of(0)
    (summed,) = run(combine_kernel, "combine", [((8 * experts, part), BF16)], [], own, one, two, three)
    returned = exchange(summed.reshape(experts, 8, part), SP).reshape(8 * experts, part)

    grad_down = jnp.einsum("rf,rd->fd", hidden_units, rows_grad, preferred_element_type=F32)
    grad_gate_w = jnp.einsum("rd,rf->df", rows_in, grad_gate_pre, preferred_element_type=F32)
    grad_up_w = jnp.einsum("rd,rf->df", rows_in, grad_up_pre, preferred_element_type=F32)

    (picked,) = run(pick_kernel, "pick", [((tok_count, part), BF16)], [], returned, place)
    half = keys // 2
    each = model_width // experts
    packed, grad_out, late_adj, _ = run(
        mixer_kernel,
        "mixer",
        [
            ((n_g, n_z * each + half, values), BF16),
            ((tok_count, values), F32),
            square,
            ((tok_count, model_width), BF16),
        ],
        [rank],
        picked,
        shifted(picked, 1),
        shifted(picked, 2),
        shifted(picked, 3),
        hidden_state,
        cotangent,
        gain_row,
        w_out,
        head_out,
        head_gain_row,
        query_rows,
        cum,
        cols,
    )

    got = exchange(packed, GROUP)
    packed, after_g = run(
        behind_kernel,
        "behind",
        [((n_z, each + half, values), BF16), square],
        spots,
        got,
        group_cols,
    )
    got = exchange(packed, "sp_0")
    grad_query, dk_part, dv_part, dlog_part = run(
        inner_kernel,
        "inner",
        [((tok_count, keys), BF16), ((tok_count, keys), F32), ((tok_count, values), F32), ((tok_count, keys), F32)],
        [],
        query_rows,
        key_rows,
        value_rows,
        cum,
        cols,
        first,
        state_in,
        grad_out,
    )
    grad_out_w, grad_key, grad_value, grad_log = run(
        final_kernel,
        "final",
        [((each, values), F32), ((tok_count, keys), BF16), ((tok_count, values), BF16), ((tok_count, keys), F32)],
        spots,
        got,
        z_cols,
        group_cols,
        after_g,
        key_rows,
        value_rows,
        cum,
        cols,
        late_adj,
        state_in,
        end,
        dk_part,
        dv_part,
        dlog_part,
    )
    return (
        grad_gate_w.astype(BF16)[None],
        grad_up_w.astype(BF16)[None],
        grad_down.astype(BF16)[None],
        grad_out_w,
        grad_query,
        grad_key,
        grad_value,
        grad_log,
    )


def solution(mesh):
    split = Mesh(mesh.devices.reshape(8, 4, 2, mesh.shape["tp"]), ("sp_0", "sp_1", "sp_2", "tp"))
    in_specs = (
        P(SP, None),
        P(),
        P(SP, None),
        P(SP, None),
        P(SP, None),
        P(SP, None, "tp"),
        P(SP, None, "tp"),
        P(SP, "tp", None),
        P(None, "tp"),
        P(SP, "tp"),
        P(SP, "tp"),
        P(SP, "tp"),
        P(SP, "tp"),
        P("tp"),
    )
    out_specs = (
        P(SP, None, "tp"),
        P(SP, None, "tp"),
        P(SP, "tp", None),
        P(SP, "tp"),
        P(SP, "tp"),
        P(SP, "tp"),
        P(SP, "tp"),
        P(SP, "tp"),
    )
    return jax.shard_map(body, mesh=split, in_specs=in_specs, out_specs=out_specs, check_vma=False)
```

time: 316 us -> 227 us (0.72)
  blocking collectives: 112 us -> 41.4 us
  local copies, waits for them, and re-layouts: 43.1 us -> 8.38 us
  Pallas kernels: 0 us -> 33.8 us
  starting transfers between devices: 20.9 us -> 37.7 us
  other arithmetic: 16.8 us -> 0.61 us
  between operations: 15 us -> 1.08 us
  matrix products: 24.4 us -> 18.5 us
    all_gather x6 -> x0, blocking collectives: 70.6 us -> none  [collected_together(): both, at, found = (lax.all_gather(jnp.concatenate(lines), axis), 0, {})]
    ppermute x0 -> x10, waiting for transfers between devices: none -> 44.8 us  [shifted(): lax.ppermute(array, 'tp', [((k + by) % N_TP, k) for k in range(N_TP)])]
    reduce_scatter x3 -> x0, waiting for transfers between devices: 34.7 us -> none  [own_rows(): so_far = lax.psum_scatter(so_far, axis, scatter_dimension=0, tiled=True)]
    pallas_call x0 -> x11, Pallas kernels: none -> 33.8 us  [run(): pl.pallas_call(kernel, out_shape=tuple((jax.ShapeDtypeStruct(shape, dtype...]
    mul x31 -> x0, local copies, waits for them, and re-layouts: 18.4 us -> none  [the longest x3 7.3 us: body(): route_weight[:, :, None] * cot_f[:, None, :]]
    ppermute x0 -> x10, starting transfers between devices: none -> 10 us  [shifted(): lax.ppermute(array, 'tp', [((k + by) % N_TP, k) for k in range(N_TP)])]
    all_gather x1 -> x0, waiting for transfers between devices: 8.27 us -> none  [side_by_side_2(): result = lax.all_gather(both, axis, axis=dim, tiled=True)]
    gather x3 -> x0, local copies, waits for them, and re-layouts: 7.85 us -> none  [the longest x1 3.35 us: body(): send_grad = padded_grad[source].reshape(expert_count, capacity, model_width)]
  transfers between devices with their start and end apart: 7 -> 15, of which waited for: 6 -> 9; matrix products, arithmetic and copies ran while one was open for 12% -> 10% of each run, Pallas kernels for 0% -> 7%
where the time goes in v1:
time: 227 us; the launch traced here: 226 us
  waiting for transfers between devices  84.9 us (37%)
  blocking collectives  41.4 us (18%)
  starting transfers between devices  37.7 us (17%)
  Pallas kernels  33.8 us (15%)
  matrix products  18.5 us (8%)
  local copies, waits for them, and re-layouts  8.38 us (4%)
    ppermute x10, waiting for transfers between devices, shifted(): lax.ppermute(array, 'tp', [((k + by) % N_TP, k) for k in range(N_TP)])  44.8 us
    all_to_all x1, blocking collectives, exchange(): return lax.all_to_all(array, axis, split_axis=0, concat_axis=0, tiled=True)  41.4 us
    all_to_all x5, waiting for transfers between devices, exchange(): return lax.all_to_all(array, axis, split_axis=0, concat_axis=0, tiled=True)  40.1 us
    pallas_call x11, Pallas kernels, run(): pl.pallas_call(kernel, out_shape=tuple((jax.ShapeDtypeStruct(shape, dtype...  33.8 us
    all_to_all x5, starting transfers between devices, exchange(): return lax.all_to_all(array, axis, split_axis=0, concat_axis=0, tiled=True)  27.7 us
    ppermute x10, starting transfers between devices, shifted(): lax.ppermute(array, 'tp', [((k + by) % N_TP, k) for k in range(N_TP)])  10 us
    unnamed x61, local copies, waits for them, and re-layouts  5.23 us
  transfers between devices with their start and end apart: 15, of which 9 were waited for; matrix products, arithmetic and copies ran while one was open for 10% of the time, Pallas kernels for 7%

profile of v1, /device:TPU:1, one launch (start us, length us, event | category | flops | bytes accessed | tf_op | source)
XLA Modules:
  0.0 226.4 jit_solution(4452857768223370149)
XLA Ops:
  0.7 1.5 copy.22.logits_ref
  2.2 4.6 %dispatch.1 = (bf16[512,1024]{1,0:T(8,128)(2,1)}, s32[2,128]{1,0:T(2,128)}) custom-call(s32[1]{0:T(128)} %bitcast.rank_ref, bf16[128,2048]{1,0:T(8,128)(2,1)} %hidden_ref.3, f32[1,2048]{1,0:T(1,128)} %bitcast.65, s32[2,128]{1,0:T(2,128)} %bitcast.67, f32[128,2]{1,0:T(8,128)} %copy.22.logits_ref, bf16[128,2048]{1,0:T(8,128)(2,1)} %cot_ref.3), custom_call_target="tpu_custom_call" | custom-call | tf_op jit(solution)/shard_map/dispatch/pallas_call | solution.py:40
  6.7 41.4 %all_to_all.30 = bf16[64,8,1024]{2,1,0:T(8,128)(2,1)} all-to-all(bf16[64,8,1024]{2,1,0:T(8,128)(2,1)} %bitcast.64), channel_id=1, replica_groups=mesh['sp_0'=8,'sp_1'=4,'sp_2'=2,'tp'=4] {'sp_0','sp_1','sp_2'}, dimensions={0} | all-to-all | bytes 2097152 | tf_op jit(solution)/shard_map/all_to_all | solution.py:23
  48.2 2.9 %unpack.1 = bf16[128,4096]{1,0:T(8,128)(2,1)} custom-call(s32[1]{0:T(128)} %constant.28.clone.1._, bf16[512,1024]{1,0:T(8,128)(2,1)} %bitcast.61), custom_call_target="tpu_custom_call" | custom-call | tf_op jit(solution)/shard_map/unpack/pallas_call | solution.py:40
  51.1 1.2 collective-permute-start.1
  52.3 1.5 collective-permute-start
  53.8 2.3 %local.1 = (bf16[8,144,128]{2,1,0:T(8,128)(2,1)}, f32[128,128]{1,0:T(8,128)}, f32[128,128]{1,0:T(8,128)}, f32[128,128]{1,0:T(8,128)}, f32[128,128]{1,0:T(8,128)}) custom-call(s32[1]{0:T(128)} %constant.28.clone.1._, bf16[128,128]{1,0:T(8,128)(2,1)} %key_ref.7, bf16[128,256]{1,0:T(8,128)(2,1)} %value_ref.7, f32[128,128]{1,0:T(8,128)} %log_ref.1), custom_call_target="tpu_custom_call" | custom-call | tf_op jit(solution)/shard_map/local/pallas_call | solution.py:40
  56.1 6.0 %all-to-all-start.2 = ((bf16[8,144,128]{2,1,0:T(8,128)(2,1)}), bf16[8,144,128]{2,1,0:T(8,128)(2,1)S(1)}, u32[]{:S(2)}, u32[]{:S(2)}) async-start(bf16[8,144,128]{2,1,0:T(8,128)(2,1)} %get-tuple-element.36), calls=%async_computation.2 | async-start | bytes 589824 | tf_op jit(solution)/shard_map/all_to_all | solution.py:23
  62.1 14.1 %collective-permute-done.1 = bf16[128,4096]{1,0:T(8,128)(2,1)} collective-permute-done((bf16[128,4096]{1,0:T(8,128)(2,1)}, bf16[128,4096]{1,0:T(8,128)(2,1)}, u32[]{:S(2)}, u32[]{:S(2)}) %collective-permute-start.1) | collective-permute-done | bytes 1048608 | tf_op jit(solution)/shard_map/ppermute | solution.py:27
  76.2 1.3 fusion.48
  77.7 1.8 fusion.47
  79.5 2.6 %collective-permute-start.3 = (bf16[128,2048]{1,0:T(8,128)(2,1)S(1)}, bf16[128,2048]{1,0:T(8,128)(2,1)S(1)}, u32[]{:S(2)}, u32[]{:S(2)}) collective-permute-start(bf16[128,2048]{1,0:T(8,128)(2,1)S(1)} %get-tuple-element.64), channel_id=1, source_target_pairs={{1,0},{2,1},{3,2},{0,3},{5,4},{6,5},{7,6},{4,7},{9,8},{10,9},{11,1... | collective-permute-start | bytes 1572872 | tf_op jit(solution)/shard_map/ppermute | solution.py:27
  82.1 8.1 %collective-permute-done.2 = bf16[128,2048]{1,0:T(8,128)(2,1)S(1)} collective-permute-done((bf16[128,2048]{1,0:T(8,128)(2,1)S(1)}, bf16[128,2048]{1,0:T(8,128)(2,1)S(1)}, u32[]{:S(2)}, u32[]{:S(2)}) %collective-permute-start.2) | collective-permute-done | bytes 524320 | tf_op jit(solution)/shard_map/ppermute | solution.py:27
  90.2 1.3 fusion.3
  91.8 1.3 fusion.5
  93.5 1.4 multiply_convert_fusion.1
  96.0 1.3 collective-permute-start.6
  99.2 0.7 collective-permute-start.4
  100.4 1.3 fusion.9.own_ref
  101.6 5.2 %collective-permute-done.6.three_ref = bf16[512,512]{1,0:T(8,128)(2,1)S(1)} collective-permute-done((bf16[512,512]{1,0:T(8,128)(2,1)S(1)}, bf16[512,512]{1,0:T(8,128)(2,1)S(1)}, u32[]{:S(2)}, u32[]{:S(2)}) %collective-permute-start.6) | collective-permute-done | bytes 524320 | tf_op jit(solution)/shard_map/ppermute | solution.py:27
  106.8 3.1 %collective-permute-done.5.two_ref = bf16[512,512]{1,0:T(8,128)(2,1)S(1)} collective-permute-done((bf16[512,512]{1,0:T(8,128)(2,1)S(1)}, bf16[512,512]{1,0:T(8,128)(2,1)S(1)}, u32[]{:S(2)}, u32[]{:S(2)}) %collective-permute-start.5) | collective-permute-done | bytes 524320 | tf_op jit(solution)/shard_map/ppermute | solution.py:27
  109.9 0.8 copy-done.18
  110.7 14.3 %collective-permute-done.4.one_ref = bf16[512,512]{1,0:T(8,128)(2,1)} collective-permute-done((bf16[512,512]{1,0:T(8,128)(2,1)S(1)}, bf16[512,512]{1,0:T(8,128)(2,1)}, u32[]{:S(2)}, u32[]{:S(2)}) %collective-permute-start.4) | collective-permute-done | bytes 524320 | tf_op jit(solution)/shard_map/ppermute | solution.py:27
  124.9 3.1 %combine.1 = bf16[512,512]{1,0:T(8,128)(2,1)} custom-call(s32[1]{0:T(128)} %constant.28.clone.1._, bf16[512,512]{1,0:T(8,128)(2,1)} %fusion.9.own_ref, bf16[512,512]{1,0:T(8,128)(2,1)} %collective-permute-done.4.one_ref, bf16[512,512]{1,0:T(8,128)(2,1)} %copy-done.18, bf16[512,512]{1,0:T(8,128)(2,1)} %copy-done.17), custom_call_target="tpu_custom_call" | custom-call | tf_op jit(solution)/shard_map/combine/pallas_call | solution.py:40
  128.0 7.9 %all-to-all-start.1 = ((bf16[64,8,512]{2,1,0:T(8,128)(2,1)}), bf16[64,8,512]{2,1,0:T(8,128)(2,1)S(1)}, u32[]{:S(2)}, u32[]{:S(2)}) async-start(bf16[64,8,512]{2,1,0:T(8,128)(2,1)} %bitcast.63), calls=%async_computation.1 | async-start | bytes 1048576 | tf_op jit(solution)/shard_map/all_to_all | solution.py:23
  135.9 0.6 pad_add_fusion.spot_ref
  136.5 2.1 group.1
  138.6 15.0 %all-to-all-done.1 = bf16[64,8,512]{2,1,0:T(8,128)(2,1)S(1)} async-done(((bf16[64,8,512]{2,1,0:T(8,128)(2,1)}), bf16[64,8,512]{2,1,0:T(8,128)(2,1)S(1)}, u32[]{:S(2)}, u32[]{:S(2)}) %all-to-all-start.1) | async-done | bytes 524320 | tf_op jit(solution)/shard_map/all_to_all | solution.py:23
  153.6 3.5 %all-to-all-start.3 = ((bf16[8,144,128]{2,1,0:T(8,128)(2,1)}), bf16[8,144,128]{2,1,0:T(8,128)(2,1)S(1)}, u32[]{:S(2)}, u32[]{:S(2)}) async-start(bf16[8,144,128]{2,1,0:T(8,128)(2,1)} %get-tuple-element.37), calls=%async_computation.3 | async-start | bytes 589824 | tf_op jit(solution)/shard_map/all_to_all | solution.py:23
  157.1 2.0 pick.1.own_ref
  159.1 1.5 collective-permute-start.8
  160.6 1.2 collective-permute-start.7
  161.8 6.5 %all-to-all-done.3.got_ref = bf16[8,144,128]{2,1,0:T(8,128)(2,1)S(1)} async-done(((bf16[8,144,128]{2,1,0:T(8,128)(2,1)}), bf16[8,144,128]{2,1,0:T(8,128)(2,1)S(1)}, u32[]{:S(2)}, u32[]{:S(2)}) %all-to-all-start.3) | async-done | bytes 294944 | tf_op jit(solution)/shard_map/all_to_all | solution.py:23
  168.3 0.7 copy-done.6
  169.0 3.3 %forward.1 = (f32[128,256]{1,0:T(8,128)}, f32[128,128]{1,0:T(8,128)}, f32[128,8]{1,0:T(8,128)}) custom-call(s32[2]{0:T(128)} %pad_add_fusion.spot_ref, bf16[8,144,128]{2,1,0:T(8,128)(2,1)} %copy-done.6, f32[128,128]{1,0:T(8,128)} %get-tuple-element.38.before_ref, f32[128,8]{1,0:T(8,128)} %get-tuple-element.39.group_ref.cols_ref, bf16[128,128]{1,0:T(8,128)(2,1)} %query_ref.5, ...), custom_call_target="tpu_custom_call" | custom-call | tf_op jit(solution)/shard_map/forward/pallas_call | solution.py:40
  172.4 0.6 copy-done.19
  173.1 4.5 %mixer.1 = (bf16[8,320,256]{2,1,0:T(8,128)(2,1)}, f32[128,256]{1,0:T(8,128)}, f32[128,128]{1,0:T(8,128)}, bf16[128,2048]{1,0:T(8,128)(2,1)}) custom-call(s32[1]{0:T(128)} %bitcast.rank_ref, bf16[128,512]{1,0:T(8,128)(2,1)} %pick.1.own_ref, bf16[128,512]{1,0:T(8,128)(2,1)} %copy-done.21, bf16[128,512]{1,0:T(8,128)(2,1)} %copy-done.20, ...), custom_call_target="tpu_custom_call" | custom-call | tf_op jit(solution)/shard_map/mixer/pallas_call | solution.py:40
  177.6 6.7 %all-to-all-start.4 = ((bf16[8,320,256]{2,1,0:T(8,128)(2,1)}), bf16[8,320,256]{2,1,0:T(8,128)(2,1)}, u32[]{:S(2)}, u32[]{:S(2)}) async-start(bf16[8,320,256]{2,1,0:T(8,128)(2,1)} %get-tuple-element.44), calls=%async_computation.4 | async-start | bytes 2621440 | tf_op jit(solution)/shard_map/all_to_all | solution.py:23
  184.3 3.8 %fusion.1 = bf16[1,2048,384]{2,1,0:T(8,128)(2,1)} fusion(bf16[512,384]{1,0:T(8,128)(2,1)S(1)} %get-tuple-element.60, bf16[128,2048]{1,0:T(8,128)(2,1)S(1)} %copy-done.10, bf16[128,2048]{1,0:T(8,128)(2,1)} %copy-done.23, bf16[128,2048]{1,0:T(8,128)(2,1)} %copy-done.16, bf16[128,2048]{1,0:T(8,128)(2,1)} %copy-done.13), kind=kOutput, calls=%fused_computation.4 | convolution fusion | flops 814481408 | bytes 4063232 | tf_op jit(solution)/shard_map/rd,rf->df/dot_general | solution.py:616
  188.1 14.1 %all-to-all-done.4.got_ref = bf16[8,320,256]{2,1,0:T(8,128)(2,1)} async-done(((bf16[8,320,256]{2,1,0:T(8,128)(2,1)}), bf16[8,320,256]{2,1,0:T(8,128)(2,1)}, u32[]{:S(2)}, u32[]{:S(2)}) %all-to-all-start.4) | async-done | bytes 1310752 | tf_op jit(solution)/shard_map/all_to_all | solution.py:23
  202.2 2.5 %behind.1 = (bf16[8,96,256]{2,1,0:T(8,128)(2,1)}, f32[128,128]{1,0:T(8,128)}) custom-call(s32[2]{0:T(128)} %pad_add_fusion.spot_ref, bf16[8,320,256]{2,1,0:T(8,128)(2,1)} %all-to-all-done.4.got_ref, f32[128,8]{1,0:T(8,128)} %get-tuple-element.39.group_ref.cols_ref), custom_call_target="tpu_custom_call" | custom-call | tf_op jit(solution)/shard_map/behind/pallas_call | solution.py:40
  204.7 3.7 %all-to-all-start.5 = ((bf16[8,96,256]{2,1,0:T(8,128)(2,1)}), bf16[8,96,256]{2,1,0:T(8,128)(2,1)S(1)}, u32[]{:S(2)}, u32[]{:S(2)}) async-start(bf16[8,96,256]{2,1,0:T(8,128)(2,1)} %get-tuple-element.45), calls=%async_computation.5 | async-start | bytes 786432 | tf_op jit(solution)/shard_map/all_to_all | solution.py:23
  208.4 3.9 %fusion = bf16[1,2048,384]{2,1,0:T(8,128)(2,1)} fusion(bf16[512,384]{1,0:T(8,128)(2,1)S(1)} %get-tuple-element.61, bf16[128,2048]{1,0:T(8,128)(2,1)S(1)} %copy-done.10, bf16[128,2048]{1,0:T(8,128)(2,1)} %copy-done.23, bf16[128,2048]{1,0:T(8,128)(2,1)} %copy-done.16, bf16[128,2048]{1,0:T(8,128)(2,1)} %copy-done.13), kind=kOutput, calls=%fused_computation.3 | convolution fusion | flops 814481408 | bytes 4063232 | tf_op jit(solution)/shard_map/rd,rf->df/dot_general | solution.py:615
  212.4 2.2 fusion.2
  214.6 3.2 %inner.1 = (bf16[128,128]{1,0:T(8,128)(2,1)}, f32[128,128]{1,0:T(8,128)}, f32[128,256]{1,0:T(8,128)}, f32[128,128]{1,0:T(8,128)}) custom-call(s32[1]{0:T(128)} %constant.28.clone.1._, bf16[128,128]{1,0:T(8,128)(2,1)} %query_ref.5, bf16[128,128]{1,0:T(8,128)(2,1)} %key_ref.7, bf16[128,256]{1,0:T(8,128)(2,1)} %value_ref.7, ...), custom_call_target="tpu_custom_call" | custom-call | tf_op jit(solution)/shard_map/inner/pallas_call | solution.py:40
  217.8 4.5 %all-to-all-done.5.got_ref = bf16[8,96,256]{2,1,0:T(8,128)(2,1)S(1)} async-done(((bf16[8,96,256]{2,1,0:T(8,128)(2,1)}), bf16[8,96,256]{2,1,0:T(8,128)(2,1)S(1)}, u32[]{:S(2)}, u32[]{:S(2)}) %all-to-all-start.5) | async-done | bytes 393248 | tf_op jit(solution)/shard_map/all_to_all | solution.py:23
  222.3 0.7 copy-done.4
  223.0 3.3 %final.1 = (f32[32,256]{1,0:T(8,128)}, bf16[128,128]{1,0:T(8,128)(2,1)}, bf16[128,256]{1,0:T(8,128)(2,1)}, f32[128,128]{1,0:T(8,128)}) custom-call(s32[2]{0:T(128)} %pad_add_fusion.spot_ref, bf16[8,96,256]{2,1,0:T(8,128)(2,1)} %copy-done.4, f32[128,8]{1,0:T(8,128)} %get-tuple-element.46.zcols_ref, f32[128,8]{1,0:T(8,128)} %get-tuple-element.39.group_ref.cols_ref, ...), custom_call_target="tpu_custom_call" | custom-call | tf_op jit(solution)/shard_map/final/pallas_call | solution.py:40
  (73 shorter events, 4.4 us)
Async XLA Ops:
  0.6 89.6 %copy-start = (bf16[1,2048,384]{2,1,0:T(8,128)(2,1)S(1)}, bf16[1,2048,384]{2,1,0:T(8,128)(2,1)}, u32[]{:S(2)}) copy-start(bf16[1,2048,384]{2,1,0:T(8,128)(2,1)} %param.19) | copy-start | bytes 4718596
  51.1 26.5 %copy-start.1 = (bf16[128,4096]{1,0:T(8,128)(2,1)S(1)}, bf16[128,4096]{1,0:T(8,128)(2,1)}, u32[]{:S(2)}) copy-start(bf16[128,4096]{1,0:T(8,128)(2,1)} %unpack.1) | copy-start | bytes 3145732
  51.1 25.1 %collective-permute-start.1 = (bf16[128,4096]{1,0:T(8,128)(2,1)}, bf16[128,4096]{1,0:T(8,128)(2,1)}, u32[]{:S(2)}, u32[]{:S(2)}) collective-permute-start(bf16[128,4096]{1,0:T(8,128)(2,1)} %unpack.1), channel_id=1, source_target_pairs={{3,0},{0,1},{1,2},{2,3},{7,4},{4,5},{5,6},{6,7},{11,8},{8,9},{9,10... | collective-permute-start | bytes 3145736 | tf_op jit(solution)/shard_map/ppermute | solution.py:27
  52.3 25.4 %collective-permute-start = (bf16[128,4096]{1,0:T(8,128)(2,1)}, bf16[128,4096]{1,0:T(8,128)(2,1)}, u32[]{:S(2)}, u32[]{:S(2)}) collective-permute-start(bf16[128,4096]{1,0:T(8,128)(2,1)} %unpack.1), channel_id=1, source_target_pairs={{1,0},{2,1},{3,2},{0,3},{5,4},{6,5},{7,6},{4,7},{9,8},{10,9},{11,1... | collective-permute-start | bytes 3145736 | tf_op jit(solution)/shard_map/ppermute | solution.py:27
  56.1 71.9 %all-to-all-start.2 = ((bf16[8,144,128]{2,1,0:T(8,128)(2,1)}), bf16[8,144,128]{2,1,0:T(8,128)(2,1)S(1)}, u32[]{:S(2)}, u32[]{:S(2)}) async-start(bf16[8,144,128]{2,1,0:T(8,128)(2,1)} %get-tuple-element.36), calls=%async_computation.2 | async-start | bytes 589824 | tf_op jit(solution)/shard_map/all_to_all | solution.py:23
  77.5 14.1 %copy-start.9 = (bf16[128,2048]{1,0:T(8,128)(2,1)}, bf16[128,2048]{1,0:T(8,128)(2,1)S(1)}, u32[]{:S(2)}) copy-start(bf16[128,2048]{1,0:T(8,128)(2,1)S(1)} %get-tuple-element.67) | copy-start | bytes 1572868
  77.5 15.7 %copy-start.7 = (bf16[128,2048]{1,0:T(8,128)(2,1)}, bf16[128,2048]{1,0:T(8,128)(2,1)S(1)}, u32[]{:S(2)}) copy-start(bf16[128,2048]{1,0:T(8,128)(2,1)S(1)} %get-tuple-element.66) | copy-start | bytes 1572868
  77.5 12.8 %collective-permute-start.2 = (bf16[128,2048]{1,0:T(8,128)(2,1)S(1)}, bf16[128,2048]{1,0:T(8,128)(2,1)S(1)}, u32[]{:S(2)}, u32[]{:S(2)}) collective-permute-start(bf16[128,2048]{1,0:T(8,128)(2,1)S(1)} %get-tuple-element.67), channel_id=1, source_target_pairs={{3,0},{0,1},{1,2},{2,3},{7,4},{4,5},{5,6},{6,7},{11,8},{8,9},{9,10... | collective-permute-start | bytes 1572872 | tf_op jit(solution)/shard_map/ppermute | solution.py:27
  77.7 13.9 %copy-start.13 = (bf16[128,2048]{1,0:T(8,128)(2,1)}, bf16[128,2048]{1,0:T(8,128)(2,1)S(1)}, u32[]{:S(2)}) copy-start(bf16[128,2048]{1,0:T(8,128)(2,1)S(1)} %get-tuple-element.63) | copy-start | bytes 1572868
  77.7 15.5 %copy-start.11 = (bf16[128,2048]{1,0:T(8,128)(2,1)}, bf16[128,2048]{1,0:T(8,128)(2,1)S(1)}, u32[]{:S(2)}) copy-start(bf16[128,2048]{1,0:T(8,128)(2,1)S(1)} %get-tuple-element.62) | copy-start | bytes 1572868
  79.5 12.0 %copy-start.16 = (bf16[128,2048]{1,0:T(8,128)(2,1)}, bf16[128,2048]{1,0:T(8,128)(2,1)S(1)}, u32[]{:S(2)}) copy-start(bf16[128,2048]{1,0:T(8,128)(2,1)S(1)} %get-tuple-element.65) | copy-start | bytes 1572868
  79.5 13.7 %copy-start.14 = (bf16[128,2048]{1,0:T(8,128)(2,1)}, bf16[128,2048]{1,0:T(8,128)(2,1)S(1)}, u32[]{:S(2)}) copy-start(bf16[128,2048]{1,0:T(8,128)(2,1)S(1)} %get-tuple-element.64) | copy-start | bytes 1572868
  79.5 13.6 %collective-permute-start.3 = (bf16[128,2048]{1,0:T(8,128)(2,1)S(1)}, bf16[128,2048]{1,0:T(8,128)(2,1)S(1)}, u32[]{:S(2)}, u32[]{:S(2)}) collective-permute-start(bf16[128,2048]{1,0:T(8,128)(2,1)S(1)} %get-tuple-element.64), channel_id=1, source_target_pairs={{1,0},{2,1},{3,2},{0,3},{5,4},{6,5},{7,6},{4,7},{9,8},{10,9},{11,1... | collective-permute-start | bytes 1572872 | tf_op jit(solution)/shard_map/ppermute | solution.py:27
  90.2 1.3 copy-start.23
  90.2 1.6 copy-start.3
  91.8 1.3 copy-start.26
  91.8 1.7 copy-start.22
  93.1 1.9 copy-start.28
  93.1 1.9 copy-start.24
  96.0 10.9 %collective-permute-start.6 = (bf16[512,512]{1,0:T(8,128)(2,1)S(1)}, bf16[512,512]{1,0:T(8,128)(2,1)S(1)}, u32[]{:S(2)}, u32[]{:S(2)}) collective-permute-start(bf16[512,512]{1,0:T(8,128)(2,1)S(1)} %fusion.12), channel_id=1, source_target_pairs={{1,0},{2,1},{3,2},{0,3},{5,4},{6,5},{7,6},{4,7},{9,8},{10,9},{11,1... | collective-permute-start | bytes 1572872 | tf_op jit(solution)/shard_map/ppermute | solution.py:27
  98.2 11.7 %collective-permute-start.5 = (bf16[512,512]{1,0:T(8,128)(2,1)S(1)}, bf16[512,512]{1,0:T(8,128)(2,1)S(1)}, u32[]{:S(2)}, u32[]{:S(2)}) collective-permute-start(bf16[512,512]{1,0:T(8,128)(2,1)S(1)} %fusion.11), channel_id=1, source_target_pairs={{2,0},{3,1},{0,2},{1,3},{6,4},{7,5},{4,6},{5,7},{10,8},{11,9},{8,1... | collective-permute-start | bytes 1572872 | tf_op jit(solution)/shard_map/ppermute | solution.py:27
  99.2 25.7 %collective-permute-start.4 = (bf16[512,512]{1,0:T(8,128)(2,1)S(1)}, bf16[512,512]{1,0:T(8,128)(2,1)}, u32[]{:S(2)}, u32[]{:S(2)}) collective-permute-start(bf16[512,512]{1,0:T(8,128)(2,1)S(1)} %fusion.10), channel_id=1, source_target_pairs={{3,0},{0,1},{1,2},{2,3},{7,4},{4,5},{5,6},{6,7},{11,8},{8,9},{9,10... | collective-permute-start | bytes 1572872 | tf_op jit(solution)/shard_map/ppermute | solution.py:27
  106.8 18.1 %copy-start.17 = (bf16[512,512]{1,0:T(8,128)(2,1)}, bf16[512,512]{1,0:T(8,128)(2,1)S(1)}, u32[]{:S(2)}) copy-start(bf16[512,512]{1,0:T(8,128)(2,1)S(1)} %collective-permute-done.6.three_ref) | copy-start | bytes 1572868
  109.9 0.8 copy-start.18
  128.0 8.5 %copy-start.5 = (bf16[8,144,128]{2,1,0:T(8,128)(2,1)}, bf16[8,144,128]{2,1,0:T(8,128)(2,1)S(1)}, u32[]{:S(2)}) copy-start(bf16[8,144,128]{2,1,0:T(8,128)(2,1)S(1)} %all-to-all-done.2.got_ref) | copy-start | bytes 884740
  128.0 25.6 %all-to-all-start.1 = ((bf16[64,8,512]{2,1,0:T(8,128)(2,1)}), bf16[64,8,512]{2,1,0:T(8,128)(2,1)S(1)}, u32[]{:S(2)}, u32[]{:S(2)}) async-start(bf16[64,8,512]{2,1,0:T(8,128)(2,1)} %bitcast.63), calls=%async_computation.1 | async-start | bytes 1048576 | tf_op jit(solution)/shard_map/all_to_all | solution.py:23
  153.6 3.5 %copy-start.2 = (bf16[64,8,512]{2,1,0:T(8,128)(2,1)}, bf16[64,8,512]{2,1,0:T(8,128)(2,1)S(1)}, u32[]{:S(2)}) copy-start(bf16[64,8,512]{2,1,0:T(8,128)(2,1)S(1)} %all-to-all-done.1) | copy-start | bytes 1572868
  153.6 14.7 %all-to-all-start.3 = ((bf16[8,144,128]{2,1,0:T(8,128)(2,1)}), bf16[8,144,128]{2,1,0:T(8,128)(2,1)S(1)}, u32[]{:S(2)}, u32[]{:S(2)}) async-start(bf16[8,144,128]{2,1,0:T(8,128)(2,1)} %get-tuple-element.37), calls=%async_computation.3 | async-start | bytes 589824 | tf_op jit(solution)/shard_map/all_to_all | solution.py:23
  159.1 13.2 %collective-permute-start.9 = (bf16[128,512]{1,0:T(8,128)(2,1)}, bf16[128,512]{1,0:T(8,128)(2,1)S(1)}, u32[]{:S(2)}, u32[]{:S(2)}) collective-permute-start(bf16[128,512]{1,0:T(8,128)(2,1)} %pick.1.own_ref), channel_id=1, source_target_pairs={{3,0},{0,1},{1,2},{2,3},{7,4},{4,5},{5,6},{6,7},{11,8},{8,9},{9,10... | collective-permute-start | bytes 393224 | tf_op jit(solution)/shard_map/ppermute | solution.py:27
  159.1 13.2 %collective-permute-start.8 = (bf16[128,512]{1,0:T(8,128)(2,1)}, bf16[128,512]{1,0:T(8,128)(2,1)S(1)}, u32[]{:S(2)}, u32[]{:S(2)}) collective-permute-start(bf16[128,512]{1,0:T(8,128)(2,1)} %pick.1.own_ref), channel_id=1, source_target_pairs={{2,0},{3,1},{0,2},{1,3},{6,4},{7,5},{4,6},{5,7},{10,8},{11,9},{8,1... | collective-permute-start | bytes 393224 | tf_op jit(solution)/shard_map/ppermute | solution.py:27
  160.6 11.8 %collective-permute-start.7 = (bf16[128,512]{1,0:T(8,128)(2,1)}, bf16[128,512]{1,0:T(8,128)(2,1)S(1)}, u32[]{:S(2)}, u32[]{:S(2)}) collective-permute-start(bf16[128,512]{1,0:T(8,128)(2,1)} %pick.1.own_ref), channel_id=1, source_target_pairs={{1,0},{2,1},{3,2},{0,3},{5,4},{6,5},{7,6},{4,7},{9,8},{10,9},{11,1... | collective-permute-start | bytes 393224 | tf_op jit(solution)/shard_map/ppermute | solution.py:27
  168.3 0.7 copy-start.6
  172.3 0.6 copy-start.19
  172.3 0.7 copy-start.20
  172.4 0.7 copy-start.21
  177.6 6.7 %copy-start.10 = (bf16[128,2048]{1,0:T(8,128)(2,1)S(1)}, bf16[128,2048]{1,0:T(8,128)(2,1)}, u32[]{:S(2)}) copy-start(bf16[128,2048]{1,0:T(8,128)(2,1)} %copy-done.9) | copy-start | bytes 1572868
  177.6 24.6 %all-to-all-start.4 = ((bf16[8,320,256]{2,1,0:T(8,128)(2,1)}), bf16[8,320,256]{2,1,0:T(8,128)(2,1)}, u32[]{:S(2)}, u32[]{:S(2)}) async-start(bf16[8,320,256]{2,1,0:T(8,128)(2,1)} %get-tuple-element.44), calls=%async_computation.4 | async-start | bytes 2621440 | tf_op jit(solution)/shard_map/all_to_all | solution.py:23
  204.7 17.6 %all-to-all-start.5 = ((bf16[8,96,256]{2,1,0:T(8,128)(2,1)}), bf16[8,96,256]{2,1,0:T(8,128)(2,1)S(1)}, u32[]{:S(2)}, u32[]{:S(2)}) async-start(bf16[8,96,256]{2,1,0:T(8,128)(2,1)} %get-tuple-element.45), calls=%async_computation.5 | async-start | bytes 786432 | tf_op jit(solution)/shard_map/all_to_all | solution.py:23
  208.4 4.0 %copy-start.8 = (bf16[128,2048]{1,0:T(8,128)(2,1)S(1)}, bf16[128,2048]{1,0:T(8,128)(2,1)}, u32[]{:S(2)}) copy-start(bf16[128,2048]{1,0:T(8,128)(2,1)} %copy-done.7) | copy-start | bytes 1572868
  208.4 4.0 %copy-start.12 = (bf16[128,2048]{1,0:T(8,128)(2,1)S(1)}, bf16[128,2048]{1,0:T(8,128)(2,1)}, u32[]{:S(2)}) copy-start(bf16[128,2048]{1,0:T(8,128)(2,1)} %copy-done.11) | copy-start | bytes 1572868
  208.4 4.0 %copy-start.15 = (bf16[128,2048]{1,0:T(8,128)(2,1)S(1)}, bf16[128,2048]{1,0:T(8,128)(2,1)}, u32[]{:S(2)}) copy-start(bf16[128,2048]{1,0:T(8,128)(2,1)} %copy-done.14) | copy-start | bytes 1572868
  208.4 4.0 %copy-start.25 = (bf16[128,2048]{1,0:T(8,128)(2,1)S(1)}, bf16[128,2048]{1,0:T(8,128)(2,1)}, u32[]{:S(2)}) copy-start(bf16[128,2048]{1,0:T(8,128)(2,1)} %copy-done.24) | copy-start | bytes 1572868
  208.4 4.0 %copy-start.27 = (f32[512,384]{1,0:T(8,128)S(1)}, f32[512,384]{1,0:T(8,128)}, u32[]{:S(2)}) copy-start(f32[512,384]{1,0:T(8,128)} %copy-done.26) | copy-start | bytes 2359300
  208.4 4.0 %copy-start.29 = (f32[512,384]{1,0:T(8,128)S(1)}, f32[512,384]{1,0:T(8,128)}, u32[]{:S(2)}) copy-start(f32[512,384]{1,0:T(8,128)} %copy-done.28) | copy-start | bytes 2359300
  222.3 0.7 copy-start.4

commit v2 on v1

--- a/solution.py
+++ b/solution.py
@@ -1,3 +1,5 @@
+from typing import NamedTuple
+
 import jax
 import jax.numpy as jnp
 from jax import lax
@@ -6,6 +8,7 @@
 from jax.sharding import Mesh
 from jax.sharding import PartitionSpec as P
 
+
 KEY_DIM = 64
 VAL_DIM = 128
 BLOCK = 64
@@ -13,8 +16,10 @@
 GROUP = ("sp_1", "sp_2")
 N_TP = 4
 N_Z = 8
+N_Y = 4
 HIGH = lax.Precision.HIGHEST
 EPS = 1e-06
+VMEM_LIMIT = 16 * 1024 * 1024
 F32 = jnp.float32
 BF16 = jnp.bfloat16
 
@@ -35,15 +40,35 @@
     return pl.BlockSpec(memory_space=pltpu.SMEM)
 
 
-def run(kernel, name, outs, numbers, *arrays):
-    numbers = jnp.stack(numbers) if numbers else jnp.zeros((1,), jnp.int32)
+class Near(NamedTuple):
+    array: jax.Array
+
+
+def run(kernel, outs, spots, *arrays, after=(), scratch=(), far=0):
+    count = 1 + len(arrays)
+
+    def call(*refs):
+        kernel(*refs[:count], *refs[count + len(after) :])
+
+    arrays = [
+        pltpu.with_memory_space_constraint(a.array, pltpu.VMEM) if isinstance(a, Near) else a
+        for a in arrays
+    ]
+
     return pl.pallas_call(
-        kernel,
-        out_shape=tuple(jax.ShapeDtypeStruct(shape, dtype) for shape, dtype in outs),
-        in_specs=[scalars()] + [whole()] * len(arrays),
+        call,
+        out_shape=tuple(
+            pltpu.VMEM(shape, dtype) if rest else jax.ShapeDtypeStruct(shape, dtype)
+            for shape, dtype, *rest in outs
+        ),
+        in_specs=[scalars()]
+        + [whole()] * (len(arrays) - far)
+        + [pl.BlockSpec(memory_space=pltpu.HBM)] * far
+        + [pl.BlockSpec(memory_space=pltpu.HBM)] * len(after),
         out_specs=tuple(whole() for _ in outs),
-        name=name,
-    )(numbers, *arrays)
+        scratch_shapes=list(scratch),
+        compiler_params=pltpu.CompilerParams(vmem_limit_bytes=VMEM_LIMIT),
+    )(spots, *arrays, *[pltpu.with_memory_space_constraint(a, pltpu.HBM) for a in after])
 
 
 def iota(shape, dim):
@@ -63,28 +88,11 @@
     return lax.dot_general(a, b, (dims, ((), ())), preferred_element_type=F32)
 
 
-def dispatch_kernel(rank_ref, hidden_ref, gain_ref, ids_ref, logits_ref, cot_ref, send_ref, place_ref):
-    rank = rank_ref[0]
-    tok, width = hidden_ref.shape
-    quarter = width // 4
-    state = hidden_ref[...].astype(F32)
-    scale = lax.rsqrt(jnp.mean(state * state, axis=-1, keepdims=True) + EPS)
-    normed = ((state * scale) * gain_ref[...]).astype(BF16)
-    logits = logits_ref[...]
-    l0, l1 = logits[:, 0:1], logits[:, 1:2]
-    top = jnp.maximum(l0, l1)
-    e0, e1 = jnp.exp(l0 - top), jnp.exp(l1 - top)
-    total = e0 + e1
-    cot = cot_ref[...].astype(F32)
-    grads = [((e / total) * cot).astype(BF16) for e in (e0, e1)]
-    rows_all = send_ref.shape[0]
-    experts = rows_all // 8
-    ids = ids_ref[...]
+def slot_rows(rank, ids, experts, tok):
     eye = iota((experts, tok), 0)
     hot = [(eye == ids[r : r + 1, :]).astype(F32) for r in range(2)]
     earlier = (iota((tok, tok), 0) < iota((tok, tok), 1)).astype(F32)
     before = paired(hot[0] + hot[1], earlier, NN)
-    rows = iota((rows_all, tok), 0)
     kept, places = [], []
     for r in range(2):
         slot = jnp.sum(before * hot[r], axis=0, keepdims=True).astype(jnp.int32)
@@ -92,47 +100,134 @@
         first = 8 * ids[r : r + 1, :] + (slot & 1)
         kept.append(jnp.where(block == rank, first, -8))
         places.append(first + 2 * ((block - rank) & 3))
+    return kept, places
+
+
+def inputs_kernel(
+    rank_ref, hidden_hbm, gain_hbm, ids_hbm, send_ref, place_ref, kept_ref, hidden_ref, gain_ref, ids_ref, sems
+):
+    copies = [
+        pltpu.make_async_copy(source, target, sems.at[k])
+        for k, (source, target) in enumerate(
+            ((hidden_hbm, hidden_ref), (gain_hbm, gain_ref), (ids_hbm, ids_ref))
+        )
+    ]
+    for copy in copies:
+        copy.start()
+    for copy in copies:
+        copy.wait()
+    tok, width = hidden_ref.shape
+    quarter = width // 4
+    state = hidden_ref[...].astype(F32)
+    scale = lax.rsqrt(jnp.mean(state * state, axis=-1, keepdims=True) + EPS)
+    normed = ((state * scale) * gain_ref[...]).astype(BF16)
+    rows_all = send_ref.shape[0]
+    kept, places = slot_rows(rank_ref[4], ids_ref[...], rows_all // 8, tok)
     place_ref[...] = jnp.concatenate(places, axis=0)
-    total_in, total_grad = None, None
-    for h in range(4):
-        pick = [(rows == kept[r] + 2 * h).astype(F32) for r in range(2)]
-        lanes = slice(h * quarter, (h + 1) * quarter)
-        term = paired((pick[0] + pick[1]).astype(BF16), normed[:, lanes], NN)
-        total_in = term if total_in is None else total_in + term
-        term = paired(pick[0].astype(BF16), grads[0][:, lanes], NN)
-        term = term + paired(pick[1].astype(BF16), grads[1][:, lanes], NN)
-        total_grad = term if total_grad is None else total_grad + term
-    send_ref[:, :quarter] = total_in.astype(BF16)
-    send_ref[:, quarter:] = total_grad.astype(BF16)
-
-
-def unpack_kernel(_, got_ref, out_ref):
+    kept_ref[...] = jnp.concatenate(kept, axis=0)
+    rows = iota((rows_all, 4 * tok), 0)
+    kept = [jnp.concatenate([k + 2 * h for h in range(4)], axis=1) for k in kept]
+    pick = ((rows == kept[0]) | (rows == kept[1])).astype(F32).astype(BF16)
+    quarters = [normed[:, h * quarter : (h + 1) * quarter] for h in range(4)]
+    send_ref[...] = paired(pick, jnp.concatenate(quarters, axis=0), NN).astype(BF16)
+
+
+def grads_kernel(_, logits_ref, cot_ref, kept_ref, send_ref):
+    tok, width = cot_ref.shape
+    quarter = width // 4
+    logits = jnp.transpose(jnp.concatenate([logits_ref[...]] * 4, axis=0))
+    l0, l1 = logits[:, 0:1], logits[:, 1:2]
+    top = jnp.maximum(l0, l1)
+    e0, e1 = jnp.exp(l0 - top), jnp.exp(l1 - top)
+    norm = e0 + e1
+    cot = cot_ref[...].astype(F32)
+    grads = [((e / norm) * cot).astype(BF16) for e in (e0, e1)]
+    quarters = [g[:, h * quarter : (h + 1) * quarter] for h in range(4) for g in grads]
+    kept = [kept_ref[r : r + 1, :] + 2 * h for h in range(4) for r in range(2)]
+    pick = iota((send_ref.shape[0], 8 * tok), 0) == jnp.concatenate(kept, axis=1)
+    pick = pick.astype(F32).astype(BF16)
+    send_ref[...] = paired(pick, jnp.concatenate(quarters, axis=0), NN).astype(BF16)
+
+
+def unpack_kernel(_, got_ref, *out_refs):
     got = got_ref[...]
-    rows, width = out_ref.shape
-    quarter = width // 8
+    rows = got.shape[0] // 4
+    quarter = got.shape[1]
+    each = rows // len(out_refs)
     line = iota((rows, got.shape[0]), 0)
     col = iota((rows, got.shape[0]), 1)
+    base = col - 8 * (line >> 1) - (line & 1)
     for h in range(4):
-        pick = (col == 8 * (line >> 1) + 2 * h + (line & 1)).astype(F32).astype(BF16)
-        both = paired(pick, got, NN).astype(BF16)
-        out_ref[:, h * quarter : (h + 1) * quarter] = both[:, :quarter]
-        out_ref[:, (4 + h) * quarter : (5 + h) * quarter] = both[:, quarter:]
-
-
-def combine_kernel(_, own_ref, one_ref, two_ref, three_ref, out_ref):
-    rows = own_ref.shape[0] // 4
-    line = iota((4 * rows, rows), 0)
-    col = iota((4 * rows, rows), 1)
-    total = None
+        pick = (base == 2 * h).astype(F32).astype(BF16)
+        block = paired(pick, got, NN).astype(BF16)
+        for k, ref in enumerate(out_refs):
+            ref[:, h * quarter : (h + 1) * quarter] = block[k * each : (k + 1) * each]
+
+
+def assembled(pieces, first=0, into=None, rows=0):
+    each, width = pieces[0].shape
+    rows = into.shape[0] if into is not None else rows
+
+    def kernel(*refs):
+        out_ref, sems = refs[-2], refs[-1]
+        copies = [
+            pltpu.make_async_copy(refs[k], out_ref.at[pl.ds(first + k * each, each), :], sems.at[k])
+            for k in range(len(pieces))
+        ]
+        for copy in copies:
+            copy.start()
+        for copy in copies:
+            copy.wait()
+
+    inputs = list(pieces) + ([] if into is None else [into])
+    return pl.pallas_call(
+        kernel,
+        out_shape=jax.ShapeDtypeStruct((rows, width), BF16),
+        in_specs=[pl.BlockSpec(memory_space=pl.ANY)] * len(inputs),
+        out_specs=pl.BlockSpec(memory_space=pl.ANY),
+        scratch_shapes=[pltpu.SemaphoreType.DMA((len(pieces),))],
+        input_output_aliases={} if into is None else {len(pieces): 0},
+        compiler_params=pltpu.CompilerParams(vmem_limit_bytes=VMEM_LIMIT),
+    )(*inputs)
+
+
+def combine_kernel(_, *refs):
+    arrays, out_ref = refs[:-1], refs[-1]
+    rows = arrays[0].shape[0] // 4
+    line = iota((4 * rows, 4 * rows), 0)
+    col = iota((4 * rows, 4 * rows), 1)
+    within = col & (rows - 1)
+    spread = line == 8 * (within >> 1) + (within & 1) + 2 * (col // rows)
+    place = (0, 1, 3, 2)
+    blocks = []
     for k in range(4):
-        acc = own_ref[k * rows : (k + 1) * rows].astype(F32)
-        for by, ref in ((1, one_ref), (2, two_ref), (3, three_ref)):
-            m = (k + by) % 4
-            acc = acc + ref[m * rows : (m + 1) * rows].astype(F32)
-        spread = (line == 8 * (col >> 1) + 2 * k + (col & 1)).astype(F32).astype(BF16)
-        term = paired(spread, acc.astype(BF16), NN)
-        total = term if total is None else total + term
-    out_ref[...] = total.astype(BF16)
+        acc = None
+        for by in range(4):
+            at = place[(k + by) % 4] * rows
+            block = arrays[by][at : at + rows].astype(F32)
+            acc = block if acc is None else acc + block
+        blocks.append(acc.astype(BF16))
+    spread = spread.astype(F32).astype(BF16)
+    out_ref[...] = paired(spread, jnp.concatenate(blocks, axis=0), NN).astype(BF16)
+
+
+def weights_kernel(
+    _, in_ref, grad_ref, units_ref, gate_pre_ref, up_pre_ref, gate_ref, up_ref, down_ref
+):
+    width = gate_ref.shape[1]
+    both = jnp.concatenate([gate_pre_ref[...], up_pre_ref[...]], axis=1)
+    units = units_ref[...]
+    block = 512
+
+    def step(k, carry):
+        at = pl.ds(pl.multiple_of(k * block, block), block)
+        out = paired(in_ref[:, at], both, TN).astype(BF16)
+        gate_ref[at, :] = out[:, :width]
+        up_ref[at, :] = out[:, width:]
+        down_ref[:, at] = paired(units, grad_ref[:, at], TN).astype(BF16)
+        return carry
+
+    lax.fori_loop(0, in_ref.shape[1] // block, step, 0)
 
 
 def pick_kernel(_, returned_ref, place_ref, out_ref):
@@ -183,7 +278,7 @@
 
 
 def local_kernel(_, key_ref, value_ref, log_ref, pack_ref, cum_ref, cols_ref, first_ref, end_ref):
-    tok, keys = key_ref.shape
+    tok, _ = key_ref.shape
     logs = log_ref[...]
     t, s = iota((tok, tok), 0), iota((tok, tok), 1)
     lower = ((t >= s) & same_block(t, s)).astype(F32)
@@ -265,7 +360,6 @@
     query = query_ref[...].astype(F32)
     query_in = query * jnp.exp(cum - mid)
     key_in = key_ref[...].astype(F32) * jnp.exp(mid - cum)
-    value = value_ref[...].astype(F32)
     start = query * jnp.exp(cum)
     t, s = iota((tok, tok), 0), iota((tok, tok), 1)
     causal = (t >= s) & same_block(t, s)
@@ -275,14 +369,20 @@
         [exact(start[:BLOCK], spread_heads(state), NN), exact(start[BLOCK:], spread_heads(later), NN)],
         axis=0,
     )
-    for h in range(2):
-        lanes = slice(h * VAL_DIM, (h + 1) * VAL_DIM)
+    out_ref[...] = outside
+
+    def step(h, carry):
+        lanes = pl.ds(pl.multiple_of(h * VAL_DIM, VAL_DIM), VAL_DIM)
         scores = exact(jnp.where(lane == h, query_in, 0.0), key_in, NT)
         scores = jnp.where(causal, scores, 0.0)
-        out_ref[:, lanes] = exact(scores, value[:, lanes], NN) + outside[:, lanes]
-
-
-def head_norm(head_out, gain):
+        value = value_ref[:, lanes].astype(F32)
+        out_ref[:, lanes] = exact(scores, value, NN) + out_ref[:, lanes]
+        return carry
+
+    lax.fori_loop(0, 2, step, 0)
+
+
+def head_norm(head_out):
     normed, scale = [], []
     for h in range(2):
         x = head_out[:, h * VAL_DIM : (h + 1) * VAL_DIM]
@@ -307,12 +407,15 @@
     query_ref,
     cum_ref,
     cols_ref,
-    pack_ref,
+    give_ref,
+    keep_ref,
     grad_ref,
     adj_ref,
+    local_ref,
     mixed_ref,
+    out_scr,
 ):
-    rank = rank_ref[0]
+    rank = rank_ref[4]
     tok, width = hidden_ref.shape
     part = width // 4
     state = hidden_ref[...].astype(F32)
@@ -336,7 +439,7 @@
         grad_mix = term if grad_mix is None else grad_mix + term
     grad_mix = grad_mix.astype(BF16).astype(F32)
     head_gain = head_gain_ref[...]
-    normed, head_scale = head_norm(head_ref[...], head_gain)
+    normed, head_scale = head_norm(head_ref[...])
     out = []
     for h in range(2):
         lanes = slice(h * VAL_DIM, (h + 1) * VAL_DIM)
@@ -349,44 +452,96 @@
     early = by_head(exact(start[:BLOCK], grad[:BLOCK], TN))
     late = by_head(exact(start[BLOCK:], grad[BLOCK:], TN))
     adj_ref[...] = late
-    local = (jnp.exp(cols_ref[:, 0:1]) * late + early).astype(BF16)
+    local = jnp.exp(cols_ref[:, 0:1]) * late + early
+    local_ref[...] = local
+    local = local.astype(BF16)
     half = local.shape[0] // 2
-    n_g, rows, _ = pack_ref.shape
-    n_z = N_Z
-    each = (rows - half) // n_z
-    state_rows = jnp.concatenate([local[:half], local[half:]], axis=1)
     mixed_out = jnp.concatenate(
         [normed[h] * head_gain[:, h * VAL_DIM : (h + 1) * VAL_DIM] for h in range(2)], axis=1
     ).astype(BF16)
-    out_part = paired(mixed_ref[...], mixed_out, TN).astype(BF16)
-
-    for q in range(n_g):
-        for z in range(n_z):
-            at = (z * n_g + q) * each
-            pack_ref[q, z * each : (z + 1) * each, :] = out_part[at : at + each]
-        pack_ref[q, n_z * each :, :] = state_rows
+
+    def step(k, carry):
+        at = pl.ds(pl.multiple_of(k * part, part), part)
+        out_scr[at, :] = paired(mixed_ref[:, at], mixed_out, TN).astype(BF16)
+        return carry
+
+    lax.fori_loop(0, 4, step, 0)
+    core = rank_ref[2]
+    rows = keep_ref.shape[0]
+    each = rows // (N_Y * N_Z)
+
+    def deal(z, carry):
+        for y in range(N_Y):
+            base = (z * N_Y + y) * 2
+            at = pl.ds(pl.multiple_of((y * N_Z + z) * each, each), each)
+            mine = pl.multiple_of((base + core) * each, each)
+            other = pl.multiple_of((base + 1 - core) * each, each)
+            keep_ref[at, :] = out_scr[pl.ds(mine, each), :]
+            give_ref[at, :] = out_scr[pl.ds(other, each), :]
+        return carry
+
+    lax.fori_loop(0, N_Z, deal, 0)
+    give_ref[rows:, :] = jnp.concatenate([local[:half], local[half:]], axis=1)
 
 
 def states_of(rows):
     return jnp.concatenate([rows[:, :VAL_DIM], rows[:, VAL_DIM:]], axis=0).astype(F32)
 
 
-def behind_kernel(spot_ref, got_ref, cols_ref, pack_ref, after_ref):
-    length, rows, _ = got_ref.shape
-    n_z, each = pack_ref.shape[0], pack_ref.shape[1]
-    half = after_ref.shape[0] // 2
-    each = each - half
-    total = got_ref[0, : rows - half, :].astype(F32)
-    for k in range(1, length):
-        total = total + got_ref[k, : rows - half, :].astype(F32)
+def pair_kernel(spot_ref, keep_ref, got_ref, local_ref, cols_ref, *out_refs):
+    own_ref, parts, (near_ref, pair_ref) = out_refs[0], out_refs[1:4], out_refs[4:]
+    core, y = spot_ref[2], spot_ref[3]
+    rows = keep_ref.shape[0]
+    per = rows // N_Y
+    half = local_ref.shape[0] // 2
+    other = states_of(got_ref[rows:, :])
+    local = local_ref[...]
+    last = core == 1
+    first_term = jnp.where(last, other, local)
+    second_term = jnp.where(last, local, other)
+    near_ref[...] = jnp.where(last, 0.0, other)
+    lane = iota(cols_ref.shape, 1)
+    logs = jnp.sum(jnp.where(lane == 2 * y, cols_ref[...], 0.0), axis=1, keepdims=True)
+    pair = first_term + jnp.exp(logs) * second_term
+    pair_ref[...] = pair
+    pair = pair.astype(BF16)
+    state_rows = jnp.concatenate([pair[:half], pair[half:]], axis=1)
+    for by in range(N_Y):
+        at = pl.multiple_of(((y + by) & 3) * per, per)
+        total = keep_ref[pl.ds(at, per), :].astype(F32) + got_ref[pl.ds(at, per), :].astype(F32)
+        if by == 0:
+            own_ref[...] = total
+        else:
+            parts[by - 1][:per, :] = total.astype(BF16)
+            parts[by - 1][per:, :] = state_rows
+
+
+def behind_kernel(spot_ref, own_ref, one_ref, two_ref, three_ref, near_ref, pair_ref, cols_ref, pack_ref, after_ref):
+    core, y = spot_ref[2], spot_ref[3]
+    per = own_ref.shape[0]
+    half = near_ref.shape[0] // 2
+    each = per // N_Z
+    total = own_ref[...]
+    pairs = [pair_ref[...]]
+    for ref in (one_ref, two_ref, three_ref):
+        total = total + ref[:per, :].astype(F32)
+        pairs.append(states_of(ref[per:, :]))
     total = total.astype(BF16)
-    here, carried = walked(
-        lambda k: states_of(got_ref[k, rows - half :, :]), jnp.exp(cols_ref[...]), spot_ref[0], length, True
-    )
-    after_ref[...] = here
+    decays = jnp.exp(cols_ref[...])
+    carried = jnp.zeros(near_ref.shape, F32)
+    here = carried
+    for k in reversed(range(N_Y)):
+        here = jnp.where(y == k, carried, here)
+        term = pairs[0]
+        for by in range(1, N_Y):
+            term = jnp.where(((y - by) & 3) == k, pairs[by], term)
+        carried = (decays[:, 2 * k : 2 * k + 1] * decays[:, 2 * k + 1 : 2 * k + 2]) * carried + term
+    lane = iota(cols_ref.shape, 1)
+    logs = jnp.sum(jnp.where(lane == 2 * y + 1, cols_ref[...], 0.0), axis=1, keepdims=True)
+    after_ref[...] = near_ref[...] + jnp.where(core == 1, 1.0, jnp.exp(logs)) * here
     carried = carried.astype(BF16)
     state_rows = jnp.concatenate([carried[:half], carried[half:]], axis=1)
-    for z in range(n_z):
+    for z in range(N_Z):
         pack_ref[z, :each, :] = total[z * each : (z + 1) * each]
         pack_ref[z, each:, :] = state_rows
 
@@ -412,7 +567,7 @@
     query, key = query_ref[...].astype(F32), key_ref[...].astype(F32)
     rise, fall = jnp.exp(cum - mid), jnp.exp(mid - cum)
     query_in, key_in = query * rise, key * fall
-    value, grad = value_ref[...].astype(F32), grad_ref[...]
+    grad = grad_ref[...]
     t, s = iota((tok, tok), 0), iota((tok, tok), 1)
     causal = (t >= s) & same_block(t, s)
     lane = iota((tok, keys), 1) // KEY_DIM
@@ -422,16 +577,22 @@
         [exact(grad[:BLOCK], spread_heads(state), NT), exact(grad[BLOCK:], spread_heads(later), NT)],
         axis=0,
     )
-    dq = jnp.zeros((tok, keys), F32)
-    dk = jnp.zeros((tok, keys), F32)
-    for h in range(2):
-        lanes = slice(h * VAL_DIM, (h + 1) * VAL_DIM)
+    zero = jnp.zeros((tok, keys), F32)
+
+    def step(h, carry):
+        dq, dk = carry
+        lanes = pl.ds(pl.multiple_of(h * VAL_DIM, VAL_DIM), VAL_DIM)
         mine = lane == h
-        dots = jnp.where(causal, exact(grad[:, lanes], value[:, lanes], NT), 0.0)
+        grad_h = grad_ref[:, lanes]
+        dots = jnp.where(causal, exact(grad_h, value_ref[:, lanes].astype(F32), NT), 0.0)
         scores = jnp.where(causal, exact(jnp.where(mine, query_in, 0.0), key_in, NT), 0.0)
-        dq = jnp.where(mine, exact(dots, key_in, NN), dq)
-        dk = jnp.where(mine, exact(dots, query_in, TN), dk)
-        dv_ref[:, lanes] = exact(scores, grad[:, lanes], TN)
+        dv_ref[:, lanes] = exact(scores, grad_h, TN)
+        return (
+            jnp.where(mine, exact(dots, key_in, NN), dq),
+            jnp.where(mine, exact(dots, query_in, TN), dk),
+        )
+
+    dq, dk = lax.fori_loop(0, 2, step, (zero, zero))
     dq = rise * dq + jnp.exp(cum) * outside
     dk = fall * dk
     dq_ref[...] = dq.astype(BF16)
@@ -498,7 +659,7 @@
     dlog_ref[...] = exact(upper, terms, NN) + exact(ones, end * end_state, NT)
 
 
-def body(
+def layer(
     hidden_state,
     norm_gain,
     route_ids,
@@ -525,73 +686,68 @@
     values = value_rows.shape[1]
     gain_row = norm_gain.reshape(1, model_width)
     head_gain_row = head_gain.reshape(1, values)
-    spots = [spot_g, spot_z]
-
-    send, place = run(
-        dispatch_kernel,
-        "dispatch",
-        [((8 * experts, 2 * part), BF16), ((2, tok_count), jnp.int32)],
-        [rank],
-        hidden_state,
-        gain_row,
-        route_ids.T,
-        route_logits,
-        cotangent,
-    )
-    got = exchange(send.reshape(experts, 8, 2 * part), SP).reshape(8 * experts, 2 * part)
-    (mine,) = run(unpack_kernel, "unpack", [((2 * experts, 2 * model_width), BF16)], [], got)
-
-    square = ((keys, VAL_DIM), F32)
+    spot_c, spot_y = lax.axis_index("sp_2"), lax.axis_index("sp_1")
+    spots = jnp.stack([spot_g, spot_z, spot_c, spot_y, rank])
+
+    send_in, place, kept = run(
+        inputs_kernel,
+        [((8 * experts, part), BF16), ((2, tok_count), jnp.int32, 1), ((2, tok_count), jnp.int32, 1)],
+        spots,
+        *[
+            pltpu.with_memory_space_constraint(a, pltpu.HBM)
+            for a in (hidden_state, gain_row, route_ids.T)
+        ],
+        scratch=[
+            pltpu.VMEM((tok_count, model_width), BF16),
+            pltpu.VMEM((1, model_width), F32),
+            pltpu.VMEM((2, tok_count), jnp.int32),
+            pltpu.SemaphoreType.DMA((3,)),
+        ],
+        far=3,
+    )
+    got_in = exchange(send_in.reshape(experts, 8, part), SP).reshape(8 * experts, part)
+    (send_grad,) = run(
+        grads_kernel, [((8 * experts, part), BF16)], spots, route_logits.T, Near(cotangent), Near(kept)
+    )
+    square = ((keys, VAL_DIM), F32, 1)
     packed, cum, cols, first, end = run(
         local_kernel,
-        "local",
-        [((n_g, keys + 16, VAL_DIM), BF16), ((tok_count, keys), F32), ((keys, tok_count), F32), square, square],
-        [],
+        [
+            ((n_g, keys + 16, VAL_DIM), BF16),
+            ((tok_count, keys), F32, 1),
+            ((keys, tok_count), F32, 1),
+            square,
+            square,
+        ],
+        spots,
         key_rows,
         value_rows,
         log_decay,
     )
-    got = exchange(packed, GROUP)
-    packed, before_g, group_cols = run(
-        group_kernel,
-        "group",
-        [((n_z, keys + 16, VAL_DIM), BF16), square, ((keys, n_g), F32)],
-        spots,
-        got,
-    )
-    got = exchange(packed, "sp_0")
-    head_out, state_in, z_cols = run(
-        forward_kernel,
-        "forward",
-        [((tok_count, values), F32), square, ((keys, n_z), F32)],
-        spots,
-        got,
-        before_g,
-        group_cols,
-        query_rows,
-        key_rows,
-        value_rows,
-        cum,
-        cols,
-        first,
-    )
-
-    left = shifted(mine, -1)
-    right = shifted(mine, 1)
-    far_in = shifted(left[:, :model_width], -1)
-    far_grad = shifted(right[:, model_width:], 1)
-    rows_in = jnp.concatenate(
-        [mine[:, :model_width], right[:, :model_width], far_in, left[:, :model_width]]
-    )
-    rows_grad = jnp.concatenate(
-        [mine[:, model_width:], right[:, model_width:], far_grad, left[:, model_width:]]
-    )
+    got_grad = exchange(send_grad.reshape(experts, 8, part), SP).reshape(8 * experts, part)
+
+    def ring(got):
+        upper, lower = run(unpack_kernel, [((experts, model_width), BF16, 1)] * 2, spots, Near(got))
+        left_upper, right_lower = shifted(upper, -1), shifted(lower, 1)
+        left_lower, right_upper = shifted(lower, -1), shifted(upper, 1)
+        far = (shifted(left_upper, -1), shifted(right_lower, 1))
+        return (upper, lower, right_upper, right_lower, left_upper, left_lower), far
+
+    near_in, far_in = ring(got_in)
+    near, far = ring(got_grad)
+    got_group = exchange(packed, GROUP)
+
     gate_w, up_w, down_w = w_gate[0], w_up[0], w_down[0]
+    hidden = gate_w.shape[1]
+    rows_all = 8 * experts
+    rows_in = assembled(near_in + far_in, rows=rows_all)
     gate_pre = jnp.dot(rows_in, gate_w, preferred_element_type=F32)
     up_pre = jnp.dot(rows_in, up_w, preferred_element_type=F32)
     gate_sig = jax.nn.sigmoid(gate_pre)
     silu_gate = gate_pre * gate_sig
     hidden_units = (silu_gate * up_pre).astype(BF16)
+    rows_grad = assembled(near, rows=rows_all)
+    rows_grad = assembled(far, first=6 * experts, into=rows_grad)
     grad_hidden = jnp.einsum("rd,fd->rf", rows_grad, down_w, preferred_element_type=F32)
     grad_gate_pre = (grad_hidden * up_pre * gate_sig * (1.0 + gate_pre * (1.0 - gate_sig))).astype(BF16)
     grad_up_pre = (grad_hidden * silu_gate).astype(BF16)
@@ -608,89 +764,159 @@
     one = shifted(features_of(1), -1)
     three = shifted(features_of(3), -3)
     own = features_of(0)
-    (summed,) = run(combine_kernel, "combine", [((8 * experts, part), BF16)], [], own, one, two, three)
+    packed, before_g, group_cols = run(
+        group_kernel,
+        [((n_z, keys + 16, VAL_DIM), BF16), square, ((keys, n_g), F32, 1)],
+        spots,
+        Near(got_group),
+    )
+    got = exchange(packed, "sp_0")
+    head_out, state_in, z_cols = run(
+        forward_kernel,
+        [((tok_count, values), F32, 1), square, ((keys, n_z), F32, 1)],
+        spots,
+        Near(got),
+        Near(before_g),
+        Near(group_cols),
+        query_rows,
+        key_rows,
+        value_rows,
+        Near(cum),
+        Near(cols),
+        Near(first),
+    )
+    (summed,) = run(
+        combine_kernel,
+        [((rows_all, part), BF16)],
+        spots,
+        Near(own),
+        Near(one),
+        Near(two),
+        Near(three),
+    )
     returned = exchange(summed.reshape(experts, 8, part), SP).reshape(8 * experts, part)
 
-    grad_down = jnp.einsum("rf,rd->fd", hidden_units, rows_grad, preferred_element_type=F32)
-    grad_gate_w = jnp.einsum("rd,rf->df", rows_in, grad_gate_pre, preferred_element_type=F32)
-    grad_up_w = jnp.einsum("rd,rf->df", rows_in, grad_up_pre, preferred_element_type=F32)
-
-    (picked,) = run(pick_kernel, "pick", [((tok_count, part), BF16)], [], returned, place)
+    rows_in, rows_grad, hidden_units, grad_gate_pre, grad_up_pre, _ = lax.optimization_barrier(
+        (rows_in, rows_grad, hidden_units, grad_gate_pre, grad_up_pre, summed)
+    )
+    grad_gate_w, grad_up_w, grad_down = run(
+        weights_kernel,
+        [((model_width, hidden), BF16)] * 2 + [((hidden, model_width), BF16)],
+        spots,
+        rows_in,
+        rows_grad,
+        hidden_units,
+        grad_gate_pre,
+        grad_up_pre,
+    )
+
+    (picked,) = run(
+        pick_kernel,
+        [((tok_count, part), BF16, 1)],
+        spots,
+        Near(returned),
+        Near(place),
+        after=(grad_down, grad_gate_w, grad_up_w),
+    )
     half = keys // 2
     each = model_width // experts
-    packed, grad_out, late_adj, _ = run(
+    rows_y = model_width // 2
+    per = rows_y // N_Y
+    give, keep, grad_out, late_adj, local_adj, _ = run(
         mixer_kernel,
-        "mixer",
         [
-            ((n_g, n_z * each + half, values), BF16),
-            ((tok_count, values), F32),
+            ((rows_y + half, values), BF16, 1),
+            ((rows_y, values), BF16, 1),
+            ((tok_count, values), F32, 1),
             square,
-            ((tok_count, model_width), BF16),
+            square,
+            ((tok_count, model_width), BF16, 1),
         ],
-        [rank],
-        picked,
-        shifted(picked, 1),
-        shifted(picked, 2),
-        shifted(picked, 3),
-        hidden_state,
-        cotangent,
+        spots,
+        Near(picked),
+        Near(shifted(picked, 1)),
+        Near(shifted(picked, 2)),
+        Near(shifted(picked, 3)),
+        Near(hidden_state),
+        Near(cotangent),
         gain_row,
-        w_out,
-        head_out,
+        Near(w_out),
+        Near(head_out),
         head_gain_row,
         query_rows,
-        cum,
-        cols,
-    )
-
-    got = exchange(packed, GROUP)
+        Near(cum),
+        Near(cols),
+        scratch=[pltpu.VMEM((model_width, values), BF16)],
+    )
+
+    got = lax.ppermute(give, "sp_2", [(0, 1), (1, 0)])
+    own, one, two, three, near, pair = run(
+        pair_kernel,
+        [((per, values), F32, 1)] + [((per + half, values), BF16, 1)] * 3 + [square] * 2,
+        spots,
+        Near(keep),
+        Near(got),
+        Near(local_adj),
+        Near(group_cols),
+    )
+    one, two, three = (
+        lax.ppermute(x, "sp_1", [(k, (k + by) % N_Y) for k in range(N_Y)])
+        for by, x in ((1, one), (2, two), (3, three))
+    )
     packed, after_g = run(
         behind_kernel,
-        "behind",
         [((n_z, each + half, values), BF16), square],
         spots,
-        got,
-        group_cols,
+        Near(own),
+        Near(one),
+        Near(two),
+        Near(three),
+        Near(near),
+        Near(pair),
+        Near(group_cols),
     )
     got = exchange(packed, "sp_0")
     grad_query, dk_part, dv_part, dlog_part = run(
         inner_kernel,
-        "inner",
-        [((tok_count, keys), BF16), ((tok_count, keys), F32), ((tok_count, values), F32), ((tok_count, keys), F32)],
-        [],
+        [
+            ((tok_count, keys), BF16),
+            ((tok_count, keys), F32, 1),
+            ((tok_count, values), F32, 1),
+            ((tok_count, keys), F32, 1),
+        ],
+        spots,
         query_rows,
         key_rows,
         value_rows,
-        cum,
-        cols,
-        first,
-        state_in,
-        grad_out,
+        Near(cum),
+        Near(cols),
+        Near(first),
+        Near(state_in),
+        Near(grad_out),
     )
     grad_out_w, grad_key, grad_value, grad_log = run(
         final_kernel,
-        "final",
         [((each, values), F32), ((tok_count, keys), BF16), ((tok_count, values), BF16), ((tok_count, keys), F32)],
         spots,
-        got,
-        z_cols,
-        group_cols,
-        after_g,
-        key_rows,
-        value_rows,
-        cum,
-        cols,
-        late_adj,
-        state_in,
-        end,
-        dk_part,
-        dv_part,
-        dlog_part,
+        Near(got),
+        Near(z_cols),
+        Near(group_cols),
+        Near(after_g),
+        Near(key_rows),
+        Near(value_rows),
+        Near(cum),
+        Near(cols),
+        Near(late_adj),
+        Near(state_in),
+        Near(end),
+        Near(dk_part),
+        Near(dv_part),
+        Near(dlog_part),
     )
     return (
-        grad_gate_w.astype(BF16)[None],
-        grad_up_w.astype(BF16)[None],
-        grad_down.astype(BF16)[None],
+        grad_gate_w[None],
+        grad_up_w[None],
+        grad_down[None],
         grad_out_w,
         grad_query,
         grad_key,
@@ -727,4 +953,4 @@
         P(SP, "tp"),
         P(SP, "tp"),
     )
-    return jax.shard_map(body, mesh=split, in_specs=in_specs, out_specs=out_specs, check_vma=False)
+    return jax.shard_map(layer, mesh=split, in_specs=in_specs, out_specs=out_specs, check_vma=False)

time: 227 us -> 229 us (level); the launches traced: 226 us -> 225 us
  starting transfers between devices: 37.7 us -> 53.9 us
  blocking collectives: 41.4 us -> 30.8 us
  matrix products: 18.5 us -> 8.54 us
  local copies, waits for them, and re-layouts: 8.38 us -> 15.6 us
  waiting for transfers between devices: 84.9 us -> 78.5 us
  Pallas kernels: 33.8 us -> 36.5 us
    ppermute x10 -> x18, waiting for transfers between devices: 44.8 us -> 32.4 us  [shifted(): lax.ppermute(array, 'tp', [((k + by) % N_TP, k) for k in range(N_TP)])]
    all_to_all x1, blocking collectives: 41.4 us -> 30.8 us  [exchange(): return lax.all_to_all(array, axis, split_axis=0, concat_axis=0, tiled=True)]
    unnamed x61 -> x80, local copies, waits for them, and re-layouts: 5.23 us -> 15.5 us
    ppermute x10 -> x18, starting transfers between devices: 10 us -> 19.5 us  [shifted(): lax.ppermute(array, 'tp', [((k + by) % N_TP, k) for k in range(N_TP)])]
    dot_general x6 -> x3, matrix products: 13.9 us -> 4.76 us  [the longest x1 2.25 us: layer(): jnp.einsum('rd,fd->rf', rows_grad, down_w, preferred_element_type=F32)]
    ppermute x0 -> x4, waiting for transfers between devices: none -> 8.1 us  [the longest x3 6.52 us: layer(): lax.ppermute(x, 'sp_1', [(k, (k + by) % N_Y) for k in range(N_Y)])]
    ppermute x0 -> x4, starting transfers between devices: none -> 4.55 us  [the longest x3 3.96 us: layer(): lax.ppermute(x, 'sp_1', [(k, (k + by) % N_Y) for k in range(N_Y)])]
    slice x3 -> x0, local copies, waits for them, and re-layouts: 3.15 us -> none  [the longest x1 1.8 us: body(): right[:, model_width:]]
  transfers between devices with their start and end apart: 15 -> 27, of which waited for: 9 -> 14; matrix products, arithmetic and copies ran while one was open for 10% -> 4% of each run, Pallas kernels for 7% -> 10%
where the time goes in v2:
time: 229 us; the launch traced here: 225 us
  waiting for transfers between devices  78.5 us (34%)
  starting transfers between devices  53.9 us (24%)
  Pallas kernels  36.5 us (16%)
  blocking collectives  30.8 us (13%)
  local copies, waits for them, and re-layouts  15.6 us (7%)
  matrix products  8.54 us (4%)
    all_to_all x5, waiting for transfers between devices, exchange(): return lax.all_to_all(array, axis, split_axis=0, concat_axis=0, tiled=True)  38 us
    pallas_call x15, Pallas kernels, run(): pl.pallas_call(call, out_shape=tuple((pltpu.VMEM(shape, dtype) if rest el...  33.8 us
    ppermute x18, waiting for transfers between devices, shifted(): lax.ppermute(array, 'tp', [((k + by) % N_TP, k) for k in range(N_TP)])  32.4 us
    all_to_all x1, blocking collectives, exchange(): return lax.all_to_all(array, axis, split_axis=0, concat_axis=0, tiled=True)  30.8 us
    all_to_all x5, starting transfers between devices, exchange(): return lax.all_to_all(array, axis, split_axis=0, concat_axis=0, tiled=True)  29.8 us
    ppermute x18, starting transfers between devices, shifted(): lax.ppermute(array, 'tp', [((k + by) % N_TP, k) for k in range(N_TP)])  19.5 us
    unnamed x80, local copies, waits for them, and re-layouts  15.5 us
    ppermute x3, waiting for transfers between devices, layer(): lax.ppermute(x, 'sp_1', [(k, (k + by) % N_Y) for k in range(N_Y)])  6.52 us
  transfers between devices with their start and end apart: 27, of which 14 were waited for; matrix products, arithmetic and copies ran while one was open for 4% of the time, Pallas kernels for 10%

profile of v2, /device:TPU:1, one launch (start us, length us, event | category | flops | bytes accessed | tf_op | source)
XLA Modules:
  0.0 224.8 jit_solution(14371707137786958058)
XLA Ops:
  0.7 3.1 %shard_map.197 = (bf16[512,512]{1,0:T(8,128)(2,1)}, s32[2,128]{1,0:T(2,128)S(1)}, s32[2,128]{1,0:T(2,128)S(1)}) custom-call(s32[5]{0:T(128)S(1)} %stack.23.refs_0_, bf16[128,2048]{1,0:T(8,128)(2,1)} %refs_5_.4, f32[1,2048]{1,0:T(1,128)} %bitcast.68, s32[2,128]{1,0:T(2,128)} %bitcast.75), custom_call_target="tpu_custom_call" | custom-call | tf_op jit(solution)/shard_map/pallas_call | solution.py:58
  6.1 1.7 shard_map.200
  7.9 30.8 %all_to_all.30 = bf16[64,8,512]{2,1,0:T(8,128)(2,1)S(1)} all-to-all(bf16[64,8,512]{2,1,0:T(8,128)(2,1)S(1)} %bitcast.67), channel_id=1, replica_groups=mesh['sp_0'=8,'sp_1'=4,'sp_2'=2,'tp'=4] {'sp_0','sp_1','sp_2'}, dimensions={0} | all-to-all | bytes 1048576 | tf_op jit(solution)/shard_map/all_to_all | solution.py:28
  38.6 5.7 %all-to-all-start = ((bf16[64,8,512]{2,1,0:T(8,128)(2,1)}), bf16[64,8,512]{2,1,0:T(8,128)(2,1)S(1)}, u32[]{:S(2)}, u32[]{:S(2)}) async-start(bf16[64,8,512]{2,1,0:T(8,128)(2,1)} %bitcast.7), calls=%async_computation | async-start | bytes 1048576 | tf_op jit(solution)/shard_map/all_to_all | solution.py:28
  45.3 1.3 collective-permute-start.6
  46.6 1.5 collective-permute-start.10
  48.1 1.3 collective-permute-start.8
  49.4 12.7 %all-to-all-done = bf16[64,8,512]{2,1,0:T(8,128)(2,1)S(1)} async-done(((bf16[64,8,512]{2,1,0:T(8,128)(2,1)}), bf16[64,8,512]{2,1,0:T(8,128)(2,1)S(1)}, u32[]{:S(2)}, u32[]{:S(2)}) %all-to-all-start) | async-done | bytes 524320 | tf_op jit(solution)/shard_map/all_to_all | solution.py:28
  62.0 1.8 shard_map.198
  63.8 1.2 collective-permute-start.2
  65.0 1.5 collective-permute-start.1
  66.5 2.7 %collective-permute-start = (bf16[64,2048]{1,0:T(8,128)(2,1)}, bf16[64,2048]{1,0:T(8,128)(2,1)}, u32[]{:S(2)}, u32[]{:S(2)}) collective-permute-start(bf16[64,2048]{1,0:T(8,128)(2,1)} %get-tuple-element.56.refs_0_), channel_id=1, source_target_pairs={{1,0},{2,1},{3,2},{0,3},{5,4},{6,5},{7,6},{4,7},{9,8},{10,9},{11,1... | collective-permute-start | bytes 786440 | tf_op jit(solution)/shard_map/ppermute | solution.py:32
  69.2 3.6 %collective-permute-done.2.refs_4_ = bf16[64,2048]{1,0:T(8,128)(2,1)} collective-permute-done((bf16[64,2048]{1,0:T(8,128)(2,1)}, bf16[64,2048]{1,0:T(8,128)(2,1)}, u32[]{:S(2)}, u32[]{:S(2)}) %collective-permute-start.2) | collective-permute-done | bytes 262176 | tf_op jit(solution)/shard_map/ppermute | solution.py:32
  72.8 2.7 %collective-permute-start.5 = (bf16[64,2048]{1,0:T(8,128)(2,1)}, bf16[64,2048]{1,0:T(8,128)(2,1)}, u32[]{:S(2)}, u32[]{:S(2)}) collective-permute-start(bf16[64,2048]{1,0:T(8,128)(2,1)} %collective-permute-done.1.refs_3_), channel_id=1, source_target_pairs={{1,0},{2,1},{3,2},{0,3},{5,4},{6,5},{7,6},{4,7},{9,8},{10,9},{11,1... | collective-permute-start | bytes 786440 | tf_op jit(solution)/shard_map/ppermute | solution.py:32
  75.5 1.9 shard_map.207
  78.1 6.9 %all-to-all-start.3 = ((bf16[8,144,128]{2,1,0:T(8,128)(2,1)}), bf16[8,144,128]{2,1,0:T(8,128)(2,1)S(1)}, u32[]{:S(2)}, u32[]{:S(2)}) async-start(bf16[8,144,128]{2,1,0:T(8,128)(2,1)} %get-tuple-element.70), calls=%async_computation.3 | async-start | bytes 589824 | tf_op jit(solution)/shard_map/all_to_all | solution.py:28
  86.1 2.7 %collective-permute-start.9 = (bf16[64,2048]{1,0:T(8,128)(2,1)S(1)}, bf16[64,2048]{1,0:T(8,128)(2,1)S(1)}, u32[]{:S(2)}, u32[]{:S(2)}) collective-permute-start(bf16[64,2048]{1,0:T(8,128)(2,1)S(1)} %collective-permute-done.8.refs_3_), channel_id=1, source_target_pairs={{1,0},{2,1},{3,2},{0,3},{5,4},{6,5},{7,6},{4,7},{9,8},{10,9},{11,1... | collective-permute-start | bytes 786440 | tf_op jit(solution)/shard_map/ppermute | solution.py:32
  89.6 1.6 shard_map.199.refs_1_
  91.2 1.3 fusion.2
  92.6 1.2 fusion.4
  93.8 1.3 collective-permute-done.7.refs_0_
  95.2 2.2 multiply_convert_fusion
  98.5 2.4 %collective-permute-start.14 = (bf16[512,512]{1,0:T(8,128)(2,1)S(1)}, bf16[512,512]{1,0:T(8,128)(2,1)S(1)}, u32[]{:S(2)}, u32[]{:S(2)}) collective-permute-start(bf16[512,512]{1,0:T(8,128)(2,1)S(1)} %fusion.9), channel_id=1, source_target_pairs={{1,0},{2,1},{3,2},{0,3},{5,4},{6,5},{7,6},{4,7},{9,8},{10,9},{11,1... | collective-permute-start | bytes 1572872 | tf_op jit(solution)/shard_map/ppermute | solution.py:32
  104.5 7.9 %collective-permute-done.14.refs_4_ = bf16[512,512]{1,0:T(8,128)(2,1)S(1)} collective-permute-done((bf16[512,512]{1,0:T(8,128)(2,1)S(1)}, bf16[512,512]{1,0:T(8,128)(2,1)S(1)}, u32[]{:S(2)}, u32[]{:S(2)}) %collective-permute-start.14) | collective-permute-done | bytes 524320 | tf_op jit(solution)/shard_map/ppermute | solution.py:32
  112.5 3.0 %collective-permute-done.13.refs_3_ = bf16[512,512]{1,0:T(8,128)(2,1)S(1)} collective-permute-done((bf16[512,512]{1,0:T(8,128)(2,1)S(1)}, bf16[512,512]{1,0:T(8,128)(2,1)S(1)}, u32[]{:S(2)}, u32[]{:S(2)}) %collective-permute-start.13) | collective-permute-done | bytes 524320 | tf_op jit(solution)/shard_map/ppermute | solution.py:32
  115.5 13.1 %collective-permute-done.12.refs_2_ = bf16[512,512]{1,0:T(8,128)(2,1)S(1)} collective-permute-done((bf16[512,512]{1,0:T(8,128)(2,1)S(1)}, bf16[512,512]{1,0:T(8,128)(2,1)S(1)}, u32[]{:S(2)}, u32[]{:S(2)}) %collective-permute-start.12) | collective-permute-done | bytes 524320 | tf_op jit(solution)/shard_map/ppermute | solution.py:32
  128.5 1.9 shard_map.204
  130.4 6.6 %all-to-all-start.2 = ((bf16[64,8,512]{2,1,0:T(8,128)(2,1)}), bf16[64,8,512]{2,1,0:T(8,128)(2,1)S(1)}, u32[]{:S(2)}, u32[]{:S(2)}) async-start(bf16[64,8,512]{2,1,0:T(8,128)(2,1)} %bitcast.26), calls=%async_computation.2 | async-start | bytes 1048576 | tf_op jit(solution)/shard_map/all_to_all | solution.py:28
  138.6 16.1 %all-to-all-done.2 = bf16[64,8,512]{2,1,0:T(8,128)(2,1)S(1)} async-done(((bf16[64,8,512]{2,1,0:T(8,128)(2,1)}), bf16[64,8,512]{2,1,0:T(8,128)(2,1)S(1)}, u32[]{:S(2)}, u32[]{:S(2)}) %all-to-all-start.2) | async-done | bytes 524320 | tf_op jit(solution)/shard_map/all_to_all | solution.py:28
  154.7 4.3 %all-to-all-start.4 = ((bf16[8,144,128]{2,1,0:T(8,128)(2,1)}), bf16[8,144,128]{2,1,0:T(8,128)(2,1)}, u32[]{:S(2)}, u32[]{:S(2)}) async-start(bf16[8,144,128]{2,1,0:T(8,128)(2,1)} %copy-done.20), calls=%async_computation.4 | async-start | bytes 589824 | tf_op jit(solution)/shard_map/all_to_all | solution.py:28
  159.0 1.6 copy-done.2
  160.6 1.6 copy-done.4
  163.2 5.9 %shard_map.205 = (bf16[2048,384]{1,0:T(8,128)(2,1)}, bf16[2048,384]{1,0:T(8,128)(2,1)}, bf16[384,2048]{1,0:T(8,128)(2,1)}) custom-call(s32[5]{0:T(128)S(1)} %stack.23.refs_0_, bf16[512,2048]{1,0:T(8,128)(2,1)S(1)} %copy-done.4, bf16[512,2048]{1,0:T(8,128)(2,1)S(1)} %copy-done.2, bf16[512,384]{1,0:T(8,128)(2,1)S(1)} %copy-done.16, ...), custom_call_target="tpu_custom_call" | custom-call | tf_op jit(solution)/shard_map/pallas_call | solution.py:58
  174.7 2.8 %shard_map.209 = (f32[128,256]{1,0:T(8,128)S(1)}, f32[128,128]{1,0:T(8,128)S(1)}, f32[128,8]{1,0:T(8,128)S(1)}) custom-call(s32[5]{0:T(128)S(1)} %stack.23.refs_0_, bf16[8,144,128]{2,1,0:T(8,128)(2,1)} %all-to-all-done.4.refs_1_, f32[128,128]{1,0:T(8,128)S(1)} %copy-done.31, f32[128,8]{1,0:T(8,128)S(1)} %copy-done.9, bf16[128,128]{1,0:T(8,128)(2,1)S(1)} %copy-done.17, ...), custom_call_target="tpu_custom_call" | custom-call | tf_op jit(solution)/shard_map/pallas_call | solution.py:58
  177.5 2.6 %collective-permute-done.17.refs_4_ = bf16[128,512]{1,0:T(8,128)(2,1)S(1)} collective-permute-done((bf16[128,512]{1,0:T(8,128)(2,1)S(1)}, bf16[128,512]{1,0:T(8,128)(2,1)S(1)}, u32[]{:S(2)}, u32[]{:S(2)}) %collective-permute-start.17) | collective-permute-done | bytes 131104 | tf_op jit(solution)/shard_map/ppermute | solution.py:32
  180.8 1.2 copy-done.12
  183.6 3.9 %shard_map.210 = (bf16[1088,256]{1,0:T(8,128)(2,1)S(1)}, bf16[1024,256]{1,0:T(8,128)(2,1)S(1)}, f32[128,256]{1,0:T(8,128)S(1)}, f32[128,128]{1,0:T(8,128)S(1)}, ...) custom-call(s32[5]{0:T(128)S(1)} %stack.23.refs_0_, bf16[128,512]{1,0:T(8,128)(2,1)S(1)} %shard_map.206.refs_1_, ...), custom_call_target="tpu_custom_call" | custom-call | tf_op jit(solution)/shard_map/pallas_call | solution.py:58
  188.1 1.6 collective-permute-done.18.refs_2_
  190.5 1.2 collective-permute-start.19
  191.7 1.2 collective-permute-start.20
  192.8 1.6 collective-permute-start.21
  194.5 3.1 %collective-permute-done.19.refs_2_ = bf16[320,256]{1,0:T(8,128)(2,1)S(1)} collective-permute-done((bf16[320,256]{1,0:T(8,128)(2,1)S(1)}, bf16[320,256]{1,0:T(8,128)(2,1)S(1)}, u32[]{:S(2)}, u32[]{:S(2)}) %collective-permute-start.19) | collective-permute-done | bytes 163872 | tf_op jit(solution)/shard_map/ppermute | solution.py:863
  197.6 2.7 %collective-permute-done.20.refs_3_ = bf16[320,256]{1,0:T(8,128)(2,1)S(1)} collective-permute-done((bf16[320,256]{1,0:T(8,128)(2,1)S(1)}, bf16[320,256]{1,0:T(8,128)(2,1)S(1)}, u32[]{:S(2)}, u32[]{:S(2)}) %collective-permute-start.20) | collective-permute-done | bytes 163872 | tf_op jit(solution)/shard_map/ppermute | solution.py:863
  201.0 1.6 shard_map.212
  202.6 6.3 %all-to-all-start.5 = ((bf16[8,96,256]{2,1,0:T(8,128)(2,1)}), bf16[8,96,256]{2,1,0:T(8,128)(2,1)S(1)}, u32[]{:S(2)}, u32[]{:S(2)}) async-start(bf16[8,96,256]{2,1,0:T(8,128)(2,1)} %get-tuple-element.87), calls=%async_computation.5 | async-start | bytes 786432 | tf_op jit(solution)/shard_map/all_to_all | solution.py:28
  209.0 3.2 %shard_map.213 = (bf16[128,128]{1,0:T(8,128)(2,1)}, f32[128,128]{1,0:T(8,128)S(1)}, f32[128,256]{1,0:T(8,128)S(1)}, f32[128,128]{1,0:T(8,128)S(1)}) custom-call(s32[5]{0:T(128)S(1)} %stack.23.refs_0_, bf16[128,128]{1,0:T(8,128)(2,1)S(1)} %copy-done.19, bf16[128,128]{1,0:T(8,128)(2,1)S(1)} %copy-done.15, bf16[128,256]{1,0:T(8,128)(2,1)S(1)} %copy-done.11, ...), custom_call_target="tpu_custom_call" | custom-call | tf_op jit(solution)/shard_map/pallas_call | solution.py:58
  212.2 9.3 %all-to-all-done.5.refs_1_ = bf16[8,96,256]{2,1,0:T(8,128)(2,1)S(1)} async-done(((bf16[8,96,256]{2,1,0:T(8,128)(2,1)}), bf16[8,96,256]{2,1,0:T(8,128)(2,1)S(1)}, u32[]{:S(2)}, u32[]{:S(2)}) %all-to-all-start.5) | async-done | bytes 393248 | tf_op jit(solution)/shard_map/all_to_all | solution.py:28
  222.3 2.5 %shard_map.214 = (f32[32,256]{1,0:T(8,128)}, bf16[128,128]{1,0:T(8,128)(2,1)}, bf16[128,256]{1,0:T(8,128)(2,1)}, f32[128,128]{1,0:T(8,128)}) custom-call(s32[5]{0:T(128)S(1)} %stack.23.refs_0_, bf16[8,96,256]{2,1,0:T(8,128)(2,1)S(1)} %all-to-all-done.5.refs_1_, f32[128,8]{1,0:T(8,128)S(1)} %get-tuple-element.88.refs_2_, f32[128,8]{1,0:T(8,128)S(1)} %copy-done.9, ...), custom_call_target="tpu_custom_call" | custom-call | tf_op jit(solution)/shard_map/pallas_call | solution.py:58
  (117 shorter events, 24.0 us)
Async XLA Ops:
  0.6 91.9 %copy-start = (bf16[1,2048,384]{2,1,0:T(8,128)(2,1)S(1)}, bf16[1,2048,384]{2,1,0:T(8,128)(2,1)}, u32[]{:S(2)}) copy-start(bf16[1,2048,384]{2,1,0:T(8,128)(2,1)} %param.19) | copy-start | bytes 4718596
  7.8 67.7 %copy-start.10 = (bf16[128,256]{1,0:T(8,128)(2,1)S(1)}, bf16[128,256]{1,0:T(8,128)(2,1)}, u32[]{:S(2)}) copy-start(bf16[128,256]{1,0:T(8,128)(2,1)} %refs_6_.5) | copy-start | bytes 196612
  7.8 67.7 %copy-start.13 = (bf16[128,128]{1,0:T(8,128)(2,1)S(1)}, bf16[128,128]{1,0:T(8,128)(2,1)}, u32[]{:S(2)}) copy-start(bf16[128,128]{1,0:T(8,128)(2,1)} %refs_5_.5) | copy-start | bytes 98308
  7.8 67.6 %copy-start.32 = (f32[128,128]{1,0:T(8,128)S(1)}, f32[128,128]{1,0:T(8,128)}, u32[]{:S(2)}) copy-start(f32[128,128]{1,0:T(8,128)} %refs_3_.2) | copy-start | bytes 196612
  38.6 23.4 %all-to-all-start = ((bf16[64,8,512]{2,1,0:T(8,128)(2,1)}), bf16[64,8,512]{2,1,0:T(8,128)(2,1)S(1)}, u32[]{:S(2)}, u32[]{:S(2)}) async-start(bf16[64,8,512]{2,1,0:T(8,128)(2,1)} %bitcast.7), calls=%async_computation | async-start | bytes 1048576 | tf_op jit(solution)/shard_map/all_to_all | solution.py:28
  45.3 21.1 %collective-permute-start.6 = (bf16[64,2048]{1,0:T(8,128)(2,1)S(1)}, bf16[64,2048]{1,0:T(8,128)(2,1)S(1)}, u32[]{:S(2)}, u32[]{:S(2)}) collective-permute-start(bf16[64,2048]{1,0:T(8,128)(2,1)S(1)} %get-tuple-element.59.refs_0_), channel_id=1, source_target_pairs={{3,0},{0,1},{1,2},{2,3},{7,4},{4,5},{5,6},{6,7},{11,8},{8,9},{9,10... | collective-permute-start | bytes 786440 | tf_op jit(solution)/shard_map/ppermute | solution.py:32
  46.6 22.5 %collective-permute-start.10 = (bf16[64,2048]{1,0:T(8,128)(2,1)S(1)}, bf16[64,2048]{1,0:T(8,128)(2,1)}, u32[]{:S(2)}, u32[]{:S(2)}) collective-permute-start(bf16[64,2048]{1,0:T(8,128)(2,1)S(1)} %get-tuple-element.59.refs_0_), channel_id=1, source_target_pairs={{1,0},{2,1},{3,2},{0,3},{5,4},{6,5},{7,6},{4,7},{9,8},{10,9},{11,1... | collective-permute-start | bytes 786440 | tf_op jit(solution)/shard_map/ppermute | solution.py:32
  48.1 18.4 %collective-permute-start.8 = (bf16[64,2048]{1,0:T(8,128)(2,1)S(1)}, bf16[64,2048]{1,0:T(8,128)(2,1)S(1)}, u32[]{:S(2)}, u32[]{:S(2)}) collective-permute-start(bf16[64,2048]{1,0:T(8,128)(2,1)S(1)} %get-tuple-element.60.refs_1_), channel_id=1, source_target_pairs={{1,0},{2,1},{3,2},{0,3},{5,4},{6,5},{7,6},{4,7},{9,8},{10,9},{11,1... | collective-permute-start | bytes 786440 | tf_op jit(solution)/shard_map/ppermute | solution.py:32
  63.8 9.0 %collective-permute-start.2 = (bf16[64,2048]{1,0:T(8,128)(2,1)}, bf16[64,2048]{1,0:T(8,128)(2,1)}, u32[]{:S(2)}, u32[]{:S(2)}) collective-permute-start(bf16[64,2048]{1,0:T(8,128)(2,1)} %get-tuple-element.56.refs_0_), channel_id=1, source_target_pairs={{3,0},{0,1},{1,2},{2,3},{7,4},{4,5},{5,6},{6,7},{11,8},{8,9},{9,10... | collective-permute-start | bytes 786440 | tf_op jit(solution)/shard_map/ppermute | solution.py:32
  65.0 7.8 %collective-permute-start.1 = (bf16[64,2048]{1,0:T(8,128)(2,1)}, bf16[64,2048]{1,0:T(8,128)(2,1)}, u32[]{:S(2)}, u32[]{:S(2)}) collective-permute-start(bf16[64,2048]{1,0:T(8,128)(2,1)} %get-tuple-element.57.refs_1_), channel_id=1, source_target_pairs={{1,0},{2,1},{3,2},{0,3},{5,4},{6,5},{7,6},{4,7},{9,8},{10,9},{11,1... | collective-permute-start | bytes 786440 | tf_op jit(solution)/shard_map/ppermute | solution.py:32
  66.5 18.5 %collective-permute-start.11 = (bf16[64,2048]{1,0:T(8,128)(2,1)S(1)}, bf16[64,2048]{1,0:T(8,128)(2,1)S(1)}, u32[]{:S(2)}, u32[]{:S(2)}) collective-permute-start(bf16[64,2048]{1,0:T(8,128)(2,1)S(1)} %get-tuple-element.60.refs_1_), channel_id=1, source_target_pairs={{3,0},{0,1},{1,2},{2,3},{7,4},{4,5},{5,6},{6,7},{11,8},{8,9},{9,10... | collective-permute-start | bytes 786440 | tf_op jit(solution)/shard_map/ppermute | solution.py:32
  66.5 19.6 %collective-permute-start = (bf16[64,2048]{1,0:T(8,128)(2,1)}, bf16[64,2048]{1,0:T(8,128)(2,1)}, u32[]{:S(2)}, u32[]{:S(2)}) collective-permute-start(bf16[64,2048]{1,0:T(8,128)(2,1)} %get-tuple-element.56.refs_0_), channel_id=1, source_target_pairs={{1,0},{2,1},{3,2},{0,3},{5,4},{6,5},{7,6},{4,7},{9,8},{10,9},{11,1... | collective-permute-start | bytes 786440 | tf_op jit(solution)/shard_map/ppermute | solution.py:32
  69.2 19.7 %collective-permute-start.3 = (bf16[64,2048]{1,0:T(8,128)(2,1)}, bf16[64,2048]{1,0:T(8,128)(2,1)}, u32[]{:S(2)}, u32[]{:S(2)}) collective-permute-start(bf16[64,2048]{1,0:T(8,128)(2,1)} %get-tuple-element.57.refs_1_), channel_id=1, source_target_pairs={{3,0},{0,1},{1,2},{2,3},{7,4},{4,5},{5,6},{6,7},{11,8},{8,9},{9,10... | collective-permute-start | bytes 786440 | tf_op jit(solution)/shard_map/ppermute | solution.py:32
  72.8 16.9 %collective-permute-start.4 = (bf16[64,2048]{1,0:T(8,128)(2,1)}, bf16[64,2048]{1,0:T(8,128)(2,1)}, u32[]{:S(2)}, u32[]{:S(2)}) collective-permute-start(bf16[64,2048]{1,0:T(8,128)(2,1)} %collective-permute-done.2.refs_4_), channel_id=1, source_target_pairs={{3,0},{0,1},{1,2},{2,3},{7,4},{4,5},{5,6},{6,7},{11,8},{8,9},{9,10... | collective-permute-start | bytes 786440 | tf_op jit(solution)/shard_map/ppermute | solution.py:32
  72.8 16.8 %collective-permute-start.5 = (bf16[64,2048]{1,0:T(8,128)(2,1)}, bf16[64,2048]{1,0:T(8,128)(2,1)}, u32[]{:S(2)}, u32[]{:S(2)}) collective-permute-start(bf16[64,2048]{1,0:T(8,128)(2,1)} %collective-permute-done.1.refs_3_), channel_id=1, source_target_pairs={{1,0},{2,1},{3,2},{0,3},{5,4},{6,5},{7,6},{4,7},{9,8},{10,9},{11,1... | collective-permute-start | bytes 786440 | tf_op jit(solution)/shard_map/ppermute | solution.py:32
  78.1 8.0 %copy-start.26 = (f32[128,128]{1,0:T(8,128)}, f32[128,128]{1,0:T(8,128)S(1)}, u32[]{:S(2)}) copy-start(f32[128,128]{1,0:T(8,128)S(1)} %get-tuple-element.92.refs_11_) | copy-start | bytes 196612
  78.1 52.4 %all-to-all-start.3 = ((bf16[8,144,128]{2,1,0:T(8,128)(2,1)}), bf16[8,144,128]{2,1,0:T(8,128)(2,1)S(1)}, u32[]{:S(2)}, u32[]{:S(2)}) async-start(bf16[8,144,128]{2,1,0:T(8,128)(2,1)} %get-tuple-element.70), calls=%async_computation.3 | async-start | bytes 589824 | tf_op jit(solution)/shard_map/all_to_all | solution.py:28
  85.0 10.2 %collective-permute-start.7 = (bf16[64,2048]{1,0:T(8,128)(2,1)S(1)}, bf16[64,2048]{1,0:T(8,128)(2,1)S(1)}, u32[]{:S(2)}, u32[]{:S(2)}) collective-permute-start(bf16[64,2048]{1,0:T(8,128)(2,1)S(1)} %collective-permute-done.6.refs_4_), channel_id=1, source_target_pairs={{3,0},{0,1},{1,2},{2,3},{7,4},{4,5},{5,6},{6,7},{11,8},{8,9},{9,10... | collective-permute-start | bytes 786440 | tf_op jit(solution)/shard_map/ppermute | solution.py:32
  86.1 5.2 %copy-start.38 = (bf16[1,2048,384]{2,1,0:T(8,128)(2,1)S(1)}, bf16[1,2048,384]{2,1,0:T(8,128)(2,1)}, u32[]{:S(2)}) copy-start(bf16[1,2048,384]{2,1,0:T(8,128)(2,1)} %param.20) | copy-start | bytes 4718596
  86.1 9.1 %collective-permute-start.9 = (bf16[64,2048]{1,0:T(8,128)(2,1)S(1)}, bf16[64,2048]{1,0:T(8,128)(2,1)S(1)}, u32[]{:S(2)}, u32[]{:S(2)}) collective-permute-start(bf16[64,2048]{1,0:T(8,128)(2,1)S(1)} %collective-permute-done.8.refs_3_), channel_id=1, source_target_pairs={{1,0},{2,1},{3,2},{0,3},{5,4},{6,5},{7,6},{4,7},{9,8},{10,9},{11,1... | collective-permute-start | bytes 786440 | tf_op jit(solution)/shard_map/ppermute | solution.py:32
  95.2 2.3 %copy-start.1 = (bf16[512,2048]{1,0:T(8,128)(2,1)}, bf16[512,2048]{1,0:T(8,128)(2,1)S(1)}, u32[]{:S(2)}) copy-start(bf16[512,2048]{1,0:T(8,128)(2,1)S(1)} %shard_map.203.refs_2_) | copy-start | bytes 6291460
  98.5 14.0 %collective-permute-start.14 = (bf16[512,512]{1,0:T(8,128)(2,1)S(1)}, bf16[512,512]{1,0:T(8,128)(2,1)S(1)}, u32[]{:S(2)}, u32[]{:S(2)}) collective-permute-start(bf16[512,512]{1,0:T(8,128)(2,1)S(1)} %fusion.9), channel_id=1, source_target_pairs={{1,0},{2,1},{3,2},{0,3},{5,4},{6,5},{7,6},{4,7},{9,8},{10,9},{11,1... | collective-permute-start | bytes 1572872 | tf_op jit(solution)/shard_map/ppermute | solution.py:32
  101.9 13.6 %collective-permute-start.13 = (bf16[512,512]{1,0:T(8,128)(2,1)S(1)}, bf16[512,512]{1,0:T(8,128)(2,1)S(1)}, u32[]{:S(2)}, u32[]{:S(2)}) collective-permute-start(bf16[512,512]{1,0:T(8,128)(2,1)S(1)} %fusion.8), channel_id=1, source_target_pairs={{2,0},{3,1},{0,2},{1,3},{6,4},{7,5},{4,6},{5,7},{10,8},{11,9},{8,1... | collective-permute-start | bytes 1572872 | tf_op jit(solution)/shard_map/ppermute | solution.py:32
  102.9 25.6 %collective-permute-start.12 = (bf16[512,512]{1,0:T(8,128)(2,1)S(1)}, bf16[512,512]{1,0:T(8,128)(2,1)S(1)}, u32[]{:S(2)}, u32[]{:S(2)}) collective-permute-start(bf16[512,512]{1,0:T(8,128)(2,1)S(1)} %fusion.7), channel_id=1, source_target_pairs={{3,0},{0,1},{1,2},{2,3},{7,4},{4,5},{5,6},{6,7},{11,8},{8,9},{9,10... | collective-permute-start | bytes 1572872 | tf_op jit(solution)/shard_map/ppermute | solution.py:32
  130.4 24.3 %all-to-all-start.2 = ((bf16[64,8,512]{2,1,0:T(8,128)(2,1)}), bf16[64,8,512]{2,1,0:T(8,128)(2,1)S(1)}, u32[]{:S(2)}, u32[]{:S(2)}) async-start(bf16[64,8,512]{2,1,0:T(8,128)(2,1)} %bitcast.26), calls=%async_computation.2 | async-start | bytes 1048576 | tf_op jit(solution)/shard_map/all_to_all | solution.py:28
  138.6 30.4 %copy-start.8 = (f32[128,8]{1,0:T(8,128)}, f32[128,8]{1,0:T(8,128)S(1)}, u32[]{:S(2)}) copy-start(f32[128,8]{1,0:T(8,128)S(1)} %get-tuple-element.73.refs_3_.refs_4_.refs_7_) | copy-start | bytes 12292
  138.6 30.4 %copy-start.30 = (f32[128,128]{1,0:T(8,128)}, f32[128,128]{1,0:T(8,128)S(1)}, u32[]{:S(2)}) copy-start(f32[128,128]{1,0:T(8,128)S(1)} %get-tuple-element.72.refs_2_) | copy-start | bytes 196612
  154.7 16.8 %all-to-all-start.4 = ((bf16[8,144,128]{2,1,0:T(8,128)(2,1)}), bf16[8,144,128]{2,1,0:T(8,128)(2,1)}, u32[]{:S(2)}, u32[]{:S(2)}) async-start(bf16[8,144,128]{2,1,0:T(8,128)(2,1)} %copy-done.20), calls=%async_computation.4 | async-start | bytes 589824 | tf_op jit(solution)/shard_map/all_to_all | solution.py:28
  163.2 5.9 %copy-start.36 = (s32[2,128]{1,0:T(2,128)S(1)}, s32[2,128]{1,0:T(2,128)}, u32[]{:S(2)}) copy-start(s32[2,128]{1,0:T(2,128)} %copy-done.35) | copy-start | bytes 3076
  169.1 2.4 %copy-start.9 = (f32[128,8]{1,0:T(8,128)S(1)}, f32[128,8]{1,0:T(8,128)}, u32[]{:S(2)}) copy-start(f32[128,8]{1,0:T(8,128)} %copy-done.8) | copy-start | bytes 12292
  169.1 2.4 %copy-start.11 = (bf16[128,256]{1,0:T(8,128)(2,1)S(1)}, bf16[128,256]{1,0:T(8,128)(2,1)}, u32[]{:S(2)}) copy-start(bf16[128,256]{1,0:T(8,128)(2,1)} %refs_6_.5) | copy-start | bytes 196612
  169.1 11.6 %copy-start.5 = (bf16[128,2048]{1,0:T(8,128)(2,1)S(1)}, bf16[128,2048]{1,0:T(8,128)(2,1)}, u32[]{:S(2)}) copy-start(bf16[128,2048]{1,0:T(8,128)(2,1)} %refs_5_.4) | copy-start | bytes 1572868
  169.1 11.6 %copy-start.7 = (bf16[128,2048]{1,0:T(8,128)(2,1)S(1)}, bf16[128,2048]{1,0:T(8,128)(2,1)}, u32[]{:S(2)}) copy-start(bf16[128,2048]{1,0:T(8,128)(2,1)} %refs_6_.4) | copy-start | bytes 1572868
  169.1 11.6 %copy-start.33 = (f32[2048]{0:T(1024)S(1)}, f32[2048]{0:T(1024)}, u32[]{:S(2)}) copy-start(f32[2048]{0:T(1024)} %param.15) | copy-start | bytes 24580
  169.1 11.6 %copy-start.34 = (f32[256]{0:T(256)S(1)}, f32[256]{0:T(256)}, u32[]{:S(2)}) copy-start(f32[256]{0:T(256)} %param.27) | copy-start | bytes 3076
  169.9 7.6 %collective-permute-start.15 = (bf16[128,512]{1,0:T(8,128)(2,1)S(1)}, bf16[128,512]{1,0:T(8,128)(2,1)S(1)}, u32[]{:S(2)}, u32[]{:S(2)}) collective-permute-start(bf16[128,512]{1,0:T(8,128)(2,1)S(1)} %shard_map.206.refs_1_), channel_id=1, source_target_pairs={{1,0},{2,1},{3,2},{0,3},{5,4},{6,5},{7,6},{4,7},{9,8},{10,9},{11,1... | collective-permute-start | bytes 393224 | tf_op jit(solution)/shard_map/ppermute | solution.py:32
  170.3 7.2 %collective-permute-start.16 = (bf16[128,512]{1,0:T(8,128)(2,1)S(1)}, bf16[128,512]{1,0:T(8,128)(2,1)S(1)}, u32[]{:S(2)}, u32[]{:S(2)}) collective-permute-start(bf16[128,512]{1,0:T(8,128)(2,1)S(1)} %shard_map.206.refs_1_), channel_id=1, source_target_pairs={{2,0},{3,1},{0,2},{1,3},{6,4},{7,5},{4,6},{5,7},{10,8},{11,9},{8,1... | collective-permute-start | bytes 393224 | tf_op jit(solution)/shard_map/ppermute | solution.py:32
  170.4 9.7 %collective-permute-start.17 = (bf16[128,512]{1,0:T(8,128)(2,1)S(1)}, bf16[128,512]{1,0:T(8,128)(2,1)S(1)}, u32[]{:S(2)}, u32[]{:S(2)}) collective-permute-start(bf16[128,512]{1,0:T(8,128)(2,1)S(1)} %shard_map.206.refs_1_), channel_id=1, source_target_pairs={{3,0},{0,1},{1,2},{2,3},{7,4},{4,5},{5,6},{6,7},{11,8},{8,9},{9,10... | collective-permute-start | bytes 393224 | tf_op jit(solution)/shard_map/ppermute | solution.py:32
  187.5 15.1 %copy-start.28 = (f32[128,128]{1,0:T(8,128)}, f32[128,128]{1,0:T(8,128)S(1)}, u32[]{:S(2)}) copy-start(f32[128,128]{1,0:T(8,128)S(1)} %get-tuple-element.90.refs_9_) | copy-start | bytes 196612
  187.5 21.4 %copy-start.15 = (bf16[128,128]{1,0:T(8,128)(2,1)S(1)}, bf16[128,128]{1,0:T(8,128)(2,1)}, u32[]{:S(2)}) copy-start(bf16[128,128]{1,0:T(8,128)(2,1)} %refs_5_.5) | copy-start | bytes 98308
  187.5 21.4 %copy-start.19 = (bf16[128,128]{1,0:T(8,128)(2,1)S(1)}, bf16[128,128]{1,0:T(8,128)(2,1)}, u32[]{:S(2)}) copy-start(bf16[128,128]{1,0:T(8,128)(2,1)} %refs_1_.5) | copy-start | bytes 98308
  187.5 21.4 %copy-start.23 = (f32[128,128]{1,0:T(8,128)S(1)}, f32[128,128]{1,0:T(8,128)}, u32[]{:S(2)}) copy-start(f32[128,128]{1,0:T(8,128)} %copy-done.21) | copy-start | bytes 196612
  187.5 2.2 collective-permute-start.18
  189.7 31.8 %copy-start.27 = (f32[128,128]{1,0:T(8,128)S(1)}, f32[128,128]{1,0:T(8,128)}, u32[]{:S(2)}) copy-start(f32[128,128]{1,0:T(8,128)} %copy-done.26) | copy-start | bytes 196612
  190.5 7.1 %collective-permute-start.19 = (bf16[320,256]{1,0:T(8,128)(2,1)S(1)}, bf16[320,256]{1,0:T(8,128)(2,1)S(1)}, u32[]{:S(2)}, u32[]{:S(2)}) collective-permute-start(bf16[320,256]{1,0:T(8,128)(2,1)S(1)} %get-tuple-element.82), channel_id=1, source_target_pairs={{0,8},{8,16},{16,24},{24,0},{1,9},{9,17},{17,25},{25,1},{2,10},{10... | collective-permute-start | bytes 491528 | tf_op jit(solution)/shard_map/ppermute | solution.py:863
  191.7 8.6 %collective-permute-start.20 = (bf16[320,256]{1,0:T(8,128)(2,1)S(1)}, bf16[320,256]{1,0:T(8,128)(2,1)S(1)}, u32[]{:S(2)}, u32[]{:S(2)}) collective-permute-start(bf16[320,256]{1,0:T(8,128)(2,1)S(1)} %get-tuple-element.83), channel_id=1, source_target_pairs={{0,16},{8,24},{16,0},{24,8},{1,17},{9,25},{17,1},{25,9},{2,18},{10... | collective-permute-start | bytes 491528 | tf_op jit(solution)/shard_map/ppermute | solution.py:863
  192.8 8.1 %collective-permute-start.21 = (bf16[320,256]{1,0:T(8,128)(2,1)S(1)}, bf16[320,256]{1,0:T(8,128)(2,1)S(1)}, u32[]{:S(2)}, u32[]{:S(2)}) collective-permute-start(bf16[320,256]{1,0:T(8,128)(2,1)S(1)} %get-tuple-element.84), channel_id=1, source_target_pairs={{0,24},{8,0},{16,8},{24,16},{1,25},{9,1},{17,9},{25,17},{2,26},{10... | collective-permute-start | bytes 491528 | tf_op jit(solution)/shard_map/ppermute | solution.py:863
  202.6 18.8 %all-to-all-start.5 = ((bf16[8,96,256]{2,1,0:T(8,128)(2,1)}), bf16[8,96,256]{2,1,0:T(8,128)(2,1)S(1)}, u32[]{:S(2)}, u32[]{:S(2)}) async-start(bf16[8,96,256]{2,1,0:T(8,128)(2,1)} %get-tuple-element.87), calls=%async_computation.5 | async-start | bytes 786432 | tf_op jit(solution)/shard_map/all_to_all | solution.py:28
  (19 other events, 18.1 us)
